TPU v7x, 32 devices: a whole 2x2x4 slice. The times are simulated.
32 devices in a mesh: kv: 8 (over z, x), tp: 4 (over y, core).
Axes of the slice: x: 2, y: 2, z: 4, core: 2. Of those that a mesh axis runs over, the one named last changes fastest.
Arguments:
- stream: bfloat16 [128, 4096], P(None, ('kv', 'tp')), may hold values from -20 to 20
- ssm_state: float32 [128, 64, 64, 128], P('kv', 'tp'), may hold values from -1.8 to 1.8
- conv_state: bfloat16 [128, 3, 8, 768], P('kv', None, 'tp'), may hold values from -6 to 6
- first_gain: float32 [4096], P(('kv', 'tp')), may hold values from 0.1 to 1.9
- first_gate: bfloat16 [4096, 11264], P('kv', 'tp'), may hold values from -0.09375 to 0.09375
- first_up: bfloat16 [4096, 11264], P('kv', 'tp'), may hold values from -0.09375 to 0.09375
- first_down: bfloat16 [11264, 4096], P('tp', 'kv'), may hold values from -0.0546875 to 0.0546875
- mix_gain: float32 [4096], P(('kv', 'tp')), may hold values from 0.1 to 1.9
- gate_in: bfloat16 [4096, 4096], P('kv', 'tp'), may hold values from -0.09375 to 0.09375
- value_in: bfloat16 [4096, 4096], P('kv', 'tp'), may hold values from -0.09375 to 0.09375
- write_in: bfloat16 [4096, 1024], P('kv', 'tp'), may hold values from -0.09375 to 0.09375
- read_in: bfloat16 [4096, 1024], P('kv', 'tp'), may hold values from -0.09375 to 0.09375
- step_in: bfloat16 [4096, 64], P('kv', 'tp'), may hold values from -0.09375 to 0.09375
- conv_weight: float32 [4, 8, 768], P(None, 'tp'), may hold values from -3 to 3
- step_bias: float32 [64], P('tp'), may hold values from -3 to 0.5
- log_decay_rate: float32 [64], P('tp'), may hold values from -1 to 2.5
- group_gain: float32 [4096], P('tp'), may hold values from 0.1 to 1.9
- out_weight: bfloat16 [4096, 4096], P('tp', 'kv'), may hold values from -0.09375 to 0.09375
- last_norm_gain: float32 [4096], P(('kv', 'tp')), may hold values from 0.1 to 1.9
- second_gate: bfloat16 [4096, 11264], P('kv', 'tp'), may hold values from -0.09375 to 0.09375
- second_up: bfloat16 [4096, 11264], P('kv', 'tp'), may hold values from -0.09375 to 0.09375
- second_down: bfloat16 [11264, 4096], P('tp', 'kv'), may hold values from -0.109375 to 0.109375
Outputs:
- next_stream: bfloat16 [128, 4096], P(None, ('kv', 'tp'))
- ssm_next: float32 [128, 64, 64, 128], P('kv', 'tp')
- conv_next: bfloat16 [128, 3, 8, 768], P('kv', None, 'tp')
All inputs are finite; a program needn't handle non-finite values.
Results may differ from a plain program's by a relative error of at most 0.015.
Values may be sent and summed in bfloat16 or wider, within the bound.
A program may use at most 128 MiB of HBM per device.

v0:
```python
import functools

import jax
import jax.numpy as jnp
from jax import lax
from jax.experimental import pallas as pl
from jax.experimental.pallas import tpu as pltpu
from jax.sharding import PartitionSpec as P

norm_epsilon = 1e-06
MESH = pl.DeviceIdType.MESH
LANES = 128
VM = pl.BlockSpec(memory_space=pltpu.VMEM)


def row_factor(total_squares, width):
    return lax.rsqrt(total_squares / width + norm_epsilon)[:, None]


def barrier(axis, n):
    me = lax.axis_index(axis)
    sem = pltpu.get_barrier_semaphore()
    for d in range(1, n):
        pl.semaphore_signal(sem, inc=1, device_id={axis: lax.rem(me + d, n)}, device_id_type=MESH)
    pl.semaphore_wait(sem, n - 1)


def remote(axis, peer, source, target, send, recv):
    return pltpu.make_async_remote_copy(
        src_ref=source,
        dst_ref=target,
        send_sem=send,
        recv_sem=recv,
        device_id={axis: peer},
        device_id_type=MESH,
    )


def block(ref, k, width, split):
    if split:
        return ref.at[k]
    return ref.at[:, pl.ds(pl.multiple_of(k * width, LANES), width)]


def scatter_start(axis, n, source_of, slots, send, recv):
    me = lax.axis_index(axis)
    copies = []
    for d in range(1, n):
        peer = lax.rem(me + d, n)
        copy = remote(axis, peer, source_of(peer), slots.at[d - 1], send.at[d - 1], recv.at[d - 1])
        copy.start()
        copies.append(copy)
    return copies


def gather(axis, n, target_of, send, recv):
    me = lax.axis_index(axis)
    copies = []
    for d in range(1, n):
        peer = lax.rem(me + d, n)
        copy = remote(axis, peer, target_of(me), target_of(me), send.at[d - 1], recv.at[d - 1])
        copy.start()
        copies.append(copy)
    for d in range(1, n):
        left = lax.rem(me - d + n, n)
        remote(axis, left, target_of(left), target_of(left), send.at[d - 1], recv.at[d - 1]).wait_recv()
    return copies


def call(kernel, outs, scratch, ident, *operands):
    return pl.pallas_call(
        kernel,
        out_shape=outs,
        in_specs=[VM] * len(operands),
        out_specs=jax.tree.map(lambda _: VM, outs),
        scratch_shapes=scratch,
        compiler_params=pltpu.CompilerParams(
            collective_id=ident, has_side_effects=True, vmem_limit_bytes=24 * 1024 * 1024
        ),
    )(*operands)


def sems(n):
    return pltpu.SemaphoreType.DMA((n - 1,))


def features_shape(rows, width, n, split):
    return (n, rows, width) if split else (rows, n * width)


def first_gather_kernel(n, split, stream_ref, gains_ref, out_ref, gains_out, s0, r0, s1, r1):
    width = stream_ref.shape[1]
    me = lax.axis_index("tp")
    if split:
        out_ref[me] = stream_ref[...]
    else:
        out_ref[:, pl.ds(pl.multiple_of(me * width, LANES), width)] = stream_ref[...]
    gains_out[me] = gains_ref[...]
    barrier("tp", n)
    copies = gather("tp", n, lambda k: block(out_ref, k, width, split), s0, r0)
    copies += gather("tp", n, lambda k: gains_out.at[k], s1, r1)
    for copy in copies:
        copy.wait_send()


def finish_kernel(n, split, weight, last, terms_ref, stream_ref, *refs):
    if last:
        after_ref, slots, s0, r0 = refs
    else:
        after_ref, out_ref, slots, s0, r0, s1, r1 = refs
    width = stream_ref.shape[1]
    me = lax.axis_index("tp")
    barrier("tp", n)
    copies = scatter_start("tp", n, lambda k: block(terms_ref, k, width, split), slots, s0, r0)
    if split:
        total = terms_ref[me].astype(jnp.float32)
    else:
        total = terms_ref[:, pl.ds(pl.multiple_of(me * width, LANES), width)].astype(jnp.float32)
    for d in range(1, n):
        copies[d - 1].wait_recv()
        total = total + slots[d - 1].astype(jnp.float32)
    after = (stream_ref[...].astype(jnp.float32) + weight * total).astype(jnp.bfloat16)
    after_ref[...] = after
    if not last:
        if split:
            out_ref[me] = after
        else:
            out_ref[:, pl.ds(pl.multiple_of(me * width, LANES), width)] = after
        copies += gather("tp", n, lambda k: block(out_ref, k, width, split), s1, r1)
    for copy in copies:
        copy.wait_send()


def hidden_kernel(n, width, gate_ref, up_ref, side_ref, out_ref, side_in, *refs):
    zn, units = gate_ref.shape[0], gate_ref.shape[3]
    near, sums, far = refs[0:2], refs[2:4], refs[4:6]
    ss, rs, sa, ra, sz, rz, sh, rh, sx, rx = refs[6:]
    parts = (gate_ref, up_ref)
    me = lax.axis_index("kv")
    z, x = me // 2, lax.rem(me, 2)
    other = z * 2 + 1 - x
    tiles = units // LANES
    cuts = [tiles * i // 4 * LANES for i in range(5)]
    ranges = [pl.ds(lo, hi - lo) for lo, hi in zip(cuts, cuts[1:])]
    barrier("kv", n)
    sides = scatter_start("kv", n, lambda k: side_ref.at[k // 2, lax.rem(k, 2)], side_in, ss, rs)
    sent = list(sides)
    first = {}
    for c, cols in enumerate(ranges):
        for i in range(2):
            copy = remote(
                "kv", other, parts[i].at[:, 1 - x, :, cols], near[i].at[:, :, cols], sa.at[c, i], ra.at[c, i]
            )
            copy.start()
            first[c, i] = copy
            sent.append(copy)
    second = {}
    for c, cols in enumerate(ranges):
        for i in range(2):
            first[c, i].wait_recv()
            total = parts[i][:, x, :, cols].astype(jnp.float32) + near[i][:, :, cols].astype(jnp.float32)
            sums[i][:, :, cols] = total.astype(jnp.bfloat16)
            for d in range(1, zn):
                zp = lax.rem(z + d, zn)
                copy = remote(
                    "kv", zp * 2 + x, sums[i].at[zp, :, cols], far[i].at[d - 1, :, cols],
                    sz.at[c, i, d - 1], rz.at[c, i, d - 1],
                )
                copy.start()
                second[c, i, d] = copy
                sent.append(copy)
    for copy in sides:
        copy.wait_recv()
    squares = side_ref[z, x]
    for d in range(n - 1):
        squares = squares + side_in[d]
    factor = lax.rsqrt(squares / width + norm_epsilon)[:, :1]

    def spread(c, d, zq, xq, peer, send, recv):
        place = out_ref.at[zq, xq, :, ranges[c]]
        return remote("kv", peer, place, place, send.at[c, d], recv.at[c, d])

    for c, cols in enumerate(ranges):
        both = []
        for i in range(2):
            total = sums[i][z, :, cols].astype(jnp.float32)
            for d in range(1, zn):
                second[c, i, d].wait_recv()
                total = total + far[i][d - 1, :, cols].astype(jnp.float32)
            both.append(total * factor)
        gate, up = both
        out_ref[z, x, :, cols] = (gate / (1.0 + jnp.exp(-gate)) * up).astype(jnp.bfloat16)
        for d in range(1, zn):
            copy = spread(c, d - 1, z, x, lax.rem(z + d, zn) * 2 + x, sh, rh)
            copy.start()
            sent.append(copy)
        copy = spread(c, 0, z, x, other, sx, rx)
        copy.start()
        sent.append(copy)
    for c in range(4):
        for d in range(1, zn):
            left = lax.rem(z - d + zn, zn)
            spread(c, d - 1, left, x, left * 2 + x, sh, rh).wait_recv()
            copy = spread(c, d, left, x, other, sx, rx)
            copy.start()
            sent.append(copy)
    for c in range(4):
        for d in range(zn):
            left = lax.rem(z - d + zn, zn)
            spread(c, d, left, 1 - x, other, sx, rx).wait_recv()
    for copy in sent:
        copy.wait_send()


def project_kernel(n, count, *refs):
    parts, outs, slots = refs[:count], refs[count : 2 * count], refs[2 * count : 3 * count]
    sem = refs[3 * count :]
    me = lax.axis_index("kv")
    barrier("kv", n)
    copies = []
    for i in range(count):
        copies.append(
            scatter_start("kv", n, lambda k, i=i: parts[i].at[k], slots[i], sem[2 * i], sem[2 * i + 1])
        )
    for i in range(count):
        for copy in copies[i]:
            copy.wait_recv()

        def tile(j, carry, i=i):
            cols = pl.ds(pl.multiple_of(j * LANES, LANES), LANES)
            total = parts[i][me, :, cols].astype(jnp.float32)
            for d in range(n - 1):
                total = total + slots[i][d, :, cols].astype(jnp.float32)
            outs[i][:, cols] = total
            return carry

        lax.fori_loop(0, outs[i].shape[1] // LANES, tile, 0)
    for group in copies:
        for copy in group:
            copy.wait_send()


def rows_gather_kernel(n, rows_ref, out_ref, s0, r0):
    out_ref[lax.axis_index("kv")] = rows_ref[...]
    barrier("kv", n)
    for copy in gather("kv", n, lambda k: out_ref.at[k], s0, r0):
        copy.wait_send()


def is_split(stream):
    return stream.shape[1] % LANES != 0


def joined(gathered, stream):
    if is_split(stream):
        return jnp.swapaxes(gathered, 0, 1).reshape(stream.shape[0], -1)
    return gathered


def normed_rows(features, gain):
    values = features.astype(jnp.float32)
    scaled = (values * gain[None]).astype(jnp.bfloat16)
    return (scaled, jnp.sum(values * values, axis=1))


def finish(stream, terms, weight, ident, last=False):
    n = lax.axis_size("tp")
    rows, width = stream.shape
    split = is_split(stream)
    terms = terms.astype(jnp.bfloat16)
    if split:
        terms = jnp.swapaxes(terms.reshape(rows, n, width), 0, 1)
    outs = [jax.ShapeDtypeStruct((rows, width), jnp.bfloat16)]
    scratch = [pltpu.VMEM((n - 1, rows, width), jnp.bfloat16), sems(n), sems(n)]
    if not last:
        outs.append(jax.ShapeDtypeStruct(features_shape(rows, width, n, split), jnp.bfloat16))
        scratch += [sems(n), sems(n)]
    result = call(
        functools.partial(finish_kernel, n, split, weight, last), outs, scratch, ident, terms, stream
    )
    if last:
        return result[0]
    return (result[0], joined(result[1], stream))


def hidden_units(features, gain, gate_weight, up_weight, ident):
    n = lax.axis_size("kv")
    rows, depth = features.shape
    count, units = rows // n, gate_weight.shape[1]
    scaled, squares = normed_rows(features, gain)
    gate = jnp.dot(scaled, gate_weight, preferred_element_type=jnp.float32).astype(jnp.bfloat16)
    up = jnp.dot(scaled, up_weight, preferred_element_type=jnp.float32).astype(jnp.bfloat16)
    side = jnp.broadcast_to(squares[:, None], (rows, LANES))
    zn = n // 2
    dma = pltpu.SemaphoreType.DMA
    hidden = call(
        functools.partial(hidden_kernel, n, depth * n),
        jax.ShapeDtypeStruct((zn, 2, count, units), jnp.bfloat16),
        [pltpu.VMEM((n - 1, count, LANES), jnp.float32)]
        + [pltpu.VMEM((zn, count, units), jnp.bfloat16)] * 4
        + [pltpu.VMEM((zn - 1, count, units), jnp.bfloat16)] * 2
        + [sems(n)] * 2
        + [dma((4, 2))] * 2
        + [dma((4, 2, zn - 1))] * 2
        + [dma((4, zn - 1))] * 2
        + [dma((4, zn))] * 2,
        ident,
        gate.reshape(zn, 2, count, units),
        up.reshape(zn, 2, count, units),
        side.reshape(zn, 2, count, LANES),
    )
    return hidden.reshape(rows, units)


def projections(features, gain, gate_in, value_in, write_in, read_in, step_in, ident):
    n = lax.axis_size("kv")
    rows = features.shape[0]
    count = rows // n
    scaled, squares = normed_rows(features, gain)
    parts = [
        jnp.dot(scaled, w, preferred_element_type=jnp.float32).astype(jnp.bfloat16)
        for w in (gate_in, value_in, write_in, read_in)
    ]
    heads = step_in.shape[1]
    step = jnp.dot(scaled, step_in, preferred_element_type=jnp.float32)
    side_width = -(-(heads + 1) // LANES) * LANES
    parts.append(
        jnp.concatenate([step, jnp.broadcast_to(squares[:, None], (rows, side_width - heads))], axis=1)
    )
    parts = [p.reshape(n, count, p.shape[1]) for p in parts]
    sums = call(
        functools.partial(project_kernel, n, len(parts)),
        [jax.ShapeDtypeStruct(p.shape[1:], jnp.float32) for p in parts],
        [pltpu.VMEM((n - 1,) + p.shape[1:], p.dtype) for p in parts] + [sems(n)] * (2 * len(parts)),
        ident,
        *parts,
    )
    return (*sums[:4], sums[4][:, :heads], sums[4][:, heads])


def rows_gather(mixed, ident):
    n = lax.axis_size("kv")
    out = call(
        functools.partial(rows_gather_kernel, n),
        jax.ShapeDtypeStruct((n,) + mixed.shape, mixed.dtype),
        [sems(n), sems(n)],
        ident,
        mixed,
    )
    return out.reshape(n * mixed.shape[0], mixed.shape[1])


def first_gather(stream, gains):
    n = lax.axis_size("tp")
    rows, width = stream.shape
    split = is_split(stream)
    packed = jnp.stack(gains)
    out, packed = call(
        functools.partial(first_gather_kernel, n, split),
        [
            jax.ShapeDtypeStruct(features_shape(rows, width, n, split), stream.dtype),
            jax.ShapeDtypeStruct((n,) + packed.shape, packed.dtype),
        ],
        [sems(n)] * 4,
        0,
        stream,
        packed,
    )
    all_gains = jnp.swapaxes(packed, 0, 1).reshape(len(gains), n * width)
    return (joined(out, stream), all_gains)


def token_mixer(
    features,
    ssm_state,
    conv_state,
    gain,
    gate_in,
    value_in,
    write_in,
    read_in,
    step_in,
    conv_weight,
    step_bias,
    log_decay_rate,
    group_gain,
    out_weight,
):
    width_all = features.shape[1] * lax.axis_size("kv")
    count = features.shape[0] // lax.axis_size("kv")
    gate_sum, value_sum, write_sum, read_sum, step_sum, total = projections(
        features, gain, gate_in, value_in, write_in, read_in, step_in, 3
    )
    factor = row_factor(total, width_all)
    gate = (gate_sum * factor).astype(jnp.bfloat16)
    values = (value_sum * factor).astype(jnp.bfloat16)
    writes = (write_sum * factor).astype(jnp.bfloat16)
    reads = (read_sum * factor).astype(jnp.bfloat16)
    steps = (step_sum * factor).astype(jnp.bfloat16)
    groups = conv_weight.shape[1]
    state_size = write_in.shape[1] // groups
    heads = step_in.shape[1]
    head_size = value_in.shape[1] // heads
    per_group = heads // groups
    width = per_group * head_size
    fresh = jnp.concatenate(
        [
            values.reshape(count, groups, width),
            writes.reshape(count, groups, state_size),
            reads.reshape(count, groups, state_size),
        ],
        axis=2,
    )
    window = jnp.concatenate([conv_state, fresh[:, None]], axis=1)
    activated = jax.nn.silu(jnp.sum(window.astype(jnp.float32) * conv_weight[None], axis=1))
    inputs = activated[:, :, :width].reshape(count, groups, per_group, head_size)
    write_vec = activated[:, :, width : width + state_size]
    read_vec = activated[:, :, width + state_size :]
    step_size = jax.nn.softplus(steps.astype(jnp.float32) + step_bias[None])
    decay = jnp.exp(-step_size * jnp.exp(log_decay_rate)[None])
    step_size = step_size.reshape(count, groups, per_group)
    decay = decay.reshape(count, groups, per_group)
    carried = ssm_state.reshape(count, groups, per_group, head_size, state_size)
    updated = (
        carried * decay[:, :, :, None, None]
        + (step_size[:, :, :, None] * inputs)[..., None] * write_vec[:, :, None, None, :]
    )
    readout = jnp.einsum("bghpn,bgn->bghp", updated, read_vec).reshape(count, groups, width)
    gated = readout * jax.nn.silu(gate.astype(jnp.float32)).reshape(count, groups, width)
    normed = gated * lax.rsqrt(jnp.mean(gated * gated, axis=2, keepdims=True) + norm_epsilon)
    mixed = (
        (normed * group_gain.reshape(groups, width)[None])
        .astype(jnp.bfloat16)
        .reshape(count, groups * width)
    )
    terms = jnp.dot(rows_gather(mixed, 4), out_weight, preferred_element_type=jnp.float32)
    return (terms, updated.reshape(ssm_state.shape), window[:, 1:])


def on_device(
    stream,
    ssm_state,
    conv_state,
    first_gain,
    first_gate,
    first_up,
    first_down,
    mix_gain,
    gate_in,
    value_in,
    write_in,
    read_in,
    step_in,
    conv_weight,
    step_bias,
    log_decay_rate,
    group_gain,
    out_weight,
    last_norm_gain,
    second_gate,
    second_up,
    second_down,
):
    features, gains = first_gather(stream, [first_gain, mix_gain, last_norm_gain])
    hidden = hidden_units(features, gains[0], first_gate, first_up, 1)
    terms = jnp.dot(hidden, first_down, preferred_element_type=jnp.float32)
    after_first, features = finish(stream, terms, 0.5, 2)
    terms, ssm_next, conv_next = token_mixer(
        features,
        ssm_state,
        conv_state,
        gains[1],
        gate_in,
        value_in,
        write_in,
        read_in,
        step_in,
        conv_weight,
        step_bias,
        log_decay_rate,
        group_gain,
        out_weight,
    )
    after_mix, features = finish(after_first, terms, 1.0, 5)
    hidden = hidden_units(features, gains[2], second_gate, second_up, 6)
    terms = jnp.dot(hidden, second_down, preferred_element_type=jnp.float32)
    next_stream = finish(after_mix, terms, 0.5, 7, last=True)
    return (next_stream, ssm_next, conv_next)


def solution(mesh):
    return jax.shard_map(
        on_device,
        mesh=mesh,
        in_specs=(
            P(None, ("kv", "tp")),
            P("kv", "tp", None, None),
            P("kv", None, "tp", None),
            P(("kv", "tp")),
            P("kv", "tp"),
            P("kv", "tp"),
            P("tp", "kv"),
            P(("kv", "tp")),
            P("kv", "tp"),
            P("kv", "tp"),
            P("kv", "tp"),
            P("kv", "tp"),
            P("kv", "tp"),
            P(None, "tp", None),
            P("tp"),
            P("tp"),
            P("tp"),
            P("tp", "kv"),
            P(("kv", "tp")),
            P("kv", "tp"),
            P("kv", "tp"),
            P("tp", "kv"),
        ),
        out_specs=(P(None, ("kv", "tp")), P("kv", "tp", None, None), P("kv", None, "tp", None)),
        check_vma=False,
    )
```

profile of v0, /device:TPU:0, one launch (start us, length us, event | category | flops | bytes accessed | tf_op | source)
XLA Modules:
  0.0 177.1 jit_solution(17226445133829151300)
XLA Ops:
  0.6 0.8 pad_maximum_fusion.1.gains_ref
  1.5 0.8 copy-done.5
  2.3 8.7 %shard_map.229 = (bf16[128,512]{1,0:T(8,128)(2,1)S(1)}, f32[4,3,128]{2,1,0:T(4,128)S(1)}) custom-call(bf16[128,128]{1,0:T(8,128)(2,1)S(1)} %copy-done.5, f32[3,128]{1,0:T(4,128)S(1)} %pad_maximum_fusion.1.gains_ref), custom_call_target="tpu_custom_call" | custom-call | tf_op jit(solution)/shard_map/pallas_call | solution.py:71
  11.1 1.4 convolution_convert_fusion.3
  12.5 1.4 convolution_convert_fusion.2
  14.2 1.1 copy-done.1
  15.3 1.1 copy-done.2
  16.4 38.4 %shard_map.230 = bf16[4,2,16,2816]{3,2,1,0:T(8,128)(2,1)S(1)} custom-call(bf16[4,2,16,2816]{3,2,1,0:T(8,128)(2,1)S(1)} %bitcast.53, bf16[4,2,16,2816]{3,2,1,0:T(8,128)(2,1)S(1)} %bitcast.54, f32[4,2,16,128]{3,2,1,0:T(8,128)S(1)} %broadcast_in_dim.13.side_ref), custom_call_target="tpu_custom_call" | custom-call | tf_op jit(solution)/shard_map/pallas_call | solution.py:71
  54.9 2.5 %convolution_convert_fusion.8.terms_ref = bf16[128,512]{1,0:T(8,128)(2,1)S(1)} fusion(bf16[128,2816]{1,0:T(8,128)(2,1)S(1)} %bitcast.51, bf16[2816,512]{1,0:T(8,128)(2,1)} %param.28), kind=kOutput, calls=%fused_computation.16 | convolution fusion | flops 369164288 | bytes 3735552 | tf_op jit(solution)/shard_map/dot_general | solution.py:466
  57.4 6.8 %shard_map.231 = (bf16[128,128]{1,0:T(8,128)(2,1)S(1)}, bf16[128,512]{1,0:T(8,128)(2,1)S(1)}) custom-call(bf16[128,512]{1,0:T(8,128)(2,1)S(1)} %convolution_convert_fusion.8.terms_ref, bf16[128,128]{1,0:T(8,128)(2,1)S(1)} %copy-done.6), custom_call_target="tpu_custom_call" | custom-call | tf_op jit(solution)/shard_map/pallas_call | solution.py:71
  64.2 0.3 convolution_convert_fusion.5
  64.6 0.3 convolution_convert_fusion.4
  65.8 21.3 %shard_map.232 = (f32[16,1024]{1,0:T(8,128)S(1)}, f32[16,1024]{1,0:T(8,128)S(1)}, f32[16,256]{1,0:T(8,128)S(1)}, f32[16,256]{1,0:T(8,128)S(1)}, f32[16,128]{1,0:T(8,128)S(1)}) custom-call(bf16[8,16,1024]{2,1,0:T(8,128)(2,1)S(1)} %bitcast.58, bf16[8,16,1024]{2,1,0:T(8,128)(2,1)S(1)} %bitcast.59, bf16[8,16,256]{2,1,0:T(8,128)(2,1)S(1)} %bitcast.60, ...), custom_call_target="tpu_custom_call" | custom-call | tf_op jit(solution)/shard_map/pallas_call | solution.py:71
  87.6 0.3 multiply_reduce_fusion
  88.0 0.6 fusion.27
  88.9 0.7 copy.30
  89.6 0.8 broadcast_multiply_fusion.1
  90.5 0.7 copy.28
  91.2 5.8 %fusion = f32[16,2,1,8,64]{4,2,3,1,0:T(1,128)S(1)} fusion(f32[16,2,128,1,1]{2,3,4,1,0:T(1,128)} %bitcast.74, f32[16,2,8,64,128]{4,3,2,1,0:T(8,128)} %bitcast.64, f32[16,2,128]{2,1,0:T(2,128)S(1)} %get-tuple-element.27, f32[16,2,8,64]{3,2,1,0:T(8,128)S(1)} %broadcast_multiply_fusion.1, f32[16,2,8]{2,1,0:T(2,128)} %copy.28), kind=kOutput, calls=%fused_computation.1 | convolution fusion | flops 10485760 | bytes 8553472 | tf_op jit(solution)/shard_map/bghpn,bgn->bghp/dot_general | solution.py:428
  97.5 8.7 %shard_map.233 = bf16[8,16,1024]{2,1,0:T(8,128)(2,1)S(1)} custom-call(bf16[16,1024]{1,0:T(8,128)(2,1)S(1)} %multiply_convert_fusion.rows_ref), custom_call_target="tpu_custom_call" | custom-call | tf_op jit(solution)/shard_map/pallas_call | solution.py:71
  106.3 1.5 convolution_convert_fusion.6.terms_ref
  107.8 7.8 %shard_map.234 = (bf16[128,128]{1,0:T(8,128)(2,1)S(1)}, bf16[128,512]{1,0:T(8,128)(2,1)S(1)}) custom-call(bf16[128,512]{1,0:T(8,128)(2,1)S(1)} %convolution_convert_fusion.6.terms_ref, bf16[128,128]{1,0:T(8,128)(2,1)S(1)} %get-tuple-element.22.stream_ref), custom_call_target="tpu_custom_call" | custom-call | tf_op jit(solution)/shard_map/pallas_call | solution.py:71
  115.6 3.2 %convolution_convert_fusion.1 = bf16[128,2816]{1,0:T(8,128)(2,1)} fusion(bf16[512,2816]{1,0:T(8,128)(2,1)} %param.41, bf16[128,512]{1,0:T(8,128)(2,1)S(1)} %get-tuple-element.23, f32[512]{0:T(512)S(1)} %bitcast.77), kind=kOutput, calls=%fused_computation.9 | convolution fusion | flops 369655808 | bytes 3737600 | tf_op jit(solution)/shard_map/dot_general | solution.py:291
  118.8 1.4 convolution_convert_fusion
  120.6 1.1 copy-done.3
  121.7 1.1 copy-done.4
  122.8 37.7 %shard_map.235 = bf16[4,2,16,2816]{3,2,1,0:T(8,128)(2,1)S(1)} custom-call(bf16[4,2,16,2816]{3,2,1,0:T(8,128)(2,1)S(1)} %bitcast.55, bf16[4,2,16,2816]{3,2,1,0:T(8,128)(2,1)S(1)} %bitcast.56, f32[4,2,16,128]{3,2,1,0:T(8,128)S(1)} %broadcast_in_dim.17.side_ref), custom_call_target="tpu_custom_call" | custom-call | tf_op jit(solution)/shard_map/pallas_call | solution.py:71
  160.5 2.4 %convolution_convert_fusion.7.terms_ref = bf16[128,512]{1,0:T(8,128)(2,1)S(1)} fusion(bf16[128,2816]{1,0:T(8,128)(2,1)S(1)} %bitcast.52, bf16[2816,512]{1,0:T(8,128)(2,1)} %param.43), kind=kOutput, calls=%fused_computation.15 | convolution fusion | flops 369164288 | bytes 3735552 | tf_op jit(solution)/shard_map/dot_general | solution.py:486
  162.8 4.2 %shard_map.236 = bf16[128,128]{1,0:T(8,128)(2,1)S(1)} custom-call(bf16[128,512]{1,0:T(8,128)(2,1)S(1)} %convolution_convert_fusion.7.terms_ref, bf16[128,128]{1,0:T(8,128)(2,1)S(1)} %get-tuple-element.24.stream_ref), custom_call_target="tpu_custom_call" | custom-call | tf_op jit(solution)/shard_map/pallas_call | solution.py:71
  167.3 8.4 %multiply_add_fusion = f32[16,16,64,128]{3,2,1,0:T(8,128)} fusion(f32[16,16,64,128]{3,2,1,0:T(8,128)} %param.23, f32[16,16,128]{2,1,0:T(8,128)S(1)} %broadcast_bitcast_fusion, f32[16,16,64]{2,1,0:T(8,128)S(1)} %broadcast_multiply_fusion, f32[16,16]{1,0:T(8,128)S(1)} %get-tuple-element.25), kind=kLoop, calls=%fused_computation | loop fusion | flops 6291456 | bytes 16974848 | tf_op jit(solution)/shard_map/add | solution.py:425
  175.6 0.9 fusion.13
  176.5 0.6 copy.36
  (70 shorter events, 3.1 us)
Async XLA Ops:
  0.6 10.4 %copy-start = (bf16[512,2816]{1,0:T(8,128)(2,1)S(1)}, bf16[512,2816]{1,0:T(8,128)(2,1)}, u32[]{:S(2)}) copy-start(bf16[512,2816]{1,0:T(8,128)(2,1)} %param.26) | copy-start | bytes 8650756
  1.5 0.8 copy-start.5
  2.3 10.2 %copy-start.7 = (bf16[512,2816]{1,0:T(8,128)(2,1)S(1)}, bf16[512,2816]{1,0:T(8,128)(2,1)}, u32[]{:S(2)}) copy-start(bf16[512,2816]{1,0:T(8,128)(2,1)} %param.27) | copy-start | bytes 8650756
  14.2 1.1 copy-start.1
  15.3 1.1 copy-start.2
  16.4 40.9 %copy-start.6 = (bf16[128,128]{1,0:T(8,128)(2,1)S(1)}, bf16[128,128]{1,0:T(8,128)(2,1)}, u32[]{:S(2)}) copy-start(bf16[128,128]{1,0:T(8,128)(2,1)} %stream_ref.3) | copy-start | bytes 98308
  16.4 47.8 %copy-start.9 = (bf16[512,1024]{1,0:T(8,128)(2,1)S(1)}, bf16[512,1024]{1,0:T(8,128)(2,1)}, u32[]{:S(2)}) copy-start(bf16[512,1024]{1,0:T(8,128)(2,1)} %param.30) | copy-start | bytes 3145732
  54.8 9.7 %copy-start.10 = (bf16[512,1024]{1,0:T(8,128)(2,1)S(1)}, bf16[512,1024]{1,0:T(8,128)(2,1)}, u32[]{:S(2)}) copy-start(bf16[512,1024]{1,0:T(8,128)(2,1)} %param.31) | copy-start | bytes 3145732
  54.8 10.1 %copy-start.12 = (bf16[512,256]{1,0:T(8,128)(2,1)S(1)}, bf16[512,256]{1,0:T(8,128)(2,1)}, u32[]{:S(2)}) copy-start(bf16[512,256]{1,0:T(8,128)(2,1)} %param.32) | copy-start | bytes 786436
  54.9 10.2 %copy-start.13 = (bf16[512,256]{1,0:T(8,128)(2,1)S(1)}, bf16[512,256]{1,0:T(8,128)(2,1)}, u32[]{:S(2)}) copy-start(bf16[512,256]{1,0:T(8,128)(2,1)} %param.33) | copy-start | bytes 786436
  57.4 8.1 %copy-start.15 = (bf16[512,16]{0,1:T(8,128)(2,1)S(1)}, bf16[512,16]{0,1:T(8,128)(2,1)}, u32[]{:S(2)}) copy-start(bf16[512,16]{0,1:T(8,128)(2,1)} %param.34) | copy-start | bytes 49156
  57.4 30.2 %copy-start.11 = (bf16[16,3,2,768]{3,2,1,0:T(2,128)(2,1)S(1)}, bf16[16,3,2,768]{3,2,1,0:T(2,128)(2,1)}, u32[]{:S(2)}) copy-start(bf16[16,3,2,768]{3,2,1,0:T(2,128)(2,1)} %param.24) | copy-start | bytes 442372
  57.4 30.2 %copy-start.14 = (f32[4,2,768]{2,1,0:T(2,128)S(1)}, f32[4,2,768]{2,1,0:T(2,128)}, u32[]{:S(2)}) copy-start(f32[4,2,768]{2,1,0:T(2,128)} %param.35) | copy-start | bytes 73732
  64.5 24.2 %copy-start.18 = (f32[16]{0:T(128)S(1)}, f32[16]{0:T(128)}, u32[]{:S(2)}) copy-start(f32[16]{0:T(128)} %param.37) | copy-start | bytes 196
  64.6 24.2 %copy-start.17 = (f32[16]{0:T(128)S(1)}, f32[16]{0:T(128)}, u32[]{:S(2)}) copy-start(f32[16]{0:T(128)} %param.36) | copy-start | bytes 196
  91.2 6.3 %copy-start.16 = (f32[1024]{0:T(1024)S(1)}, f32[1024]{0:T(1024)}, u32[]{:S(2)}) copy-start(f32[1024]{0:T(1024)} %param.38) | copy-start | bytes 12292
  97.5 21.4 %copy-start.8 = (bf16[512,2816]{1,0:T(8,128)(2,1)S(1)}, bf16[512,2816]{1,0:T(8,128)(2,1)}, u32[]{:S(2)}) copy-start(bf16[512,2816]{1,0:T(8,128)(2,1)} %param.42) | copy-start | bytes 8650756
  120.5 1.1 copy-start.3
  121.7 1.1 copy-start.4
where the time goes:
time: 178 us; the launch traced here: 177 us
  Pallas kernels  134 us (75%)
  matrix products  20.8 us (12%)
  other arithmetic  12.4 us (7%)
  local copies, waits for them, and re-layouts  9.15 us (5%)
    pallas_call x8, Pallas kernels, call(): pl.pallas_call(kernel, out_shape=outs, in_specs=[VM] * len(operands), out...  134 us
    add x1, other arithmetic, token_mixer(): carried * decay[:, :, :, None, None]  8.37 us
    unnamed x40, local copies, waits for them, and re-layouts  6 us
    dot_general x1, matrix products, token_mixer(): jnp.einsum('bghpn,bgn->bghp', updated, read_vec)  5.84 us
    dot_general x2, matrix products, hidden_units(): jnp.dot(scaled, gate_weight, preferred_element_type=jnp.float32)  4.64 us

commit v1 on v0

v1 whole, which is shorter than its diff:
```python
import functools

import jax
import jax.numpy as jnp
from jax import lax
from jax.experimental import pallas as pl
from jax.experimental.pallas import tpu as pltpu
from jax.sharding import PartitionSpec as P

norm_epsilon = 1e-06
MESH = pl.DeviceIdType.MESH
LANES = 128
VM = pl.BlockSpec(memory_space=pltpu.VMEM)
HB = pl.BlockSpec(memory_space=pltpu.HBM)
F32 = jnp.float32
BF16 = jnp.bfloat16


def sigmoid_gate(v):
    return v / (1.0 + jnp.exp(-v))


def copy_to(src, dst, send, recv, **where):
    return pltpu.make_async_remote_copy(
        src_ref=src, dst_ref=dst, send_sem=send, recv_sem=recv, device_id=where, device_id_type=MESH
    )


class Plan:
    def __init__(self):
        self.names, self.shapes = [], []

    def add(self, name, shape, dtype):
        self.names.append(name)
        self.shapes.append(pltpu.VMEM(shape, dtype))

    def sem(self, name, *shape):
        self.names.append(name)
        self.shapes.append(pltpu.SemaphoreType.DMA(shape or (1,)))


def cut(total, shares):
    ends = [0] + [max(1, round(total * s)) for s in shares] + [total]
    return [(a, b) for a, b in zip(ends, ends[1:]) if b > a]


class Sizes:
    def __init__(self, n, nt, rows, depth, units, heads, head, state, groups, split):
        self.n, self.nt, self.rows, self.depth, self.units = n, nt, rows, depth, units
        self.heads, self.head, self.state, self.groups, self.split = heads, head, state, groups, split
        self.zn, self.zh, self.ny = n // 2, n // 4, nt // 2
        self.count, self.half = rows // n, rows // 2
        tiles = units // LANES
        b = max(1, tiles // 4)
        self.ff_a = cut(tiles - b, (0.2, 0.5, 0.8))
        self.ff_b = (tiles - b, tiles)
        self.inner = heads * head
        self.group_width = self.inner // groups
        self.channels = self.group_width + 2 * state
        v, g = self.inner // LANES, self.inner // LANES
        gb = max(1, g * 5 // 8)
        vec = groups * state
        self.mix_chunks = [
            [("value", 0, v // 2 * LANES)],
            [("value", v // 2 * LANES, v * LANES), ("write", 0, vec)],
            [("read", 0, vec), ("step", 0, LANES), ("gate", gb * LANES, g * LANES)],
            [("gate", 0, gb * LANES)],
        ]
        spans, at = [], 0
        self.place = {}
        for chunk in self.mix_chunks:
            lo = at
            for name, a, z in chunk:
                self.place[name, a] = (at, z - a)
                at += z - a
            spans.append((lo, at))
        self.mix_a, self.mix_b, self.mix_width = spans[:-1], spans[-1], at


def add_sum(plan, s, p, width, bwidth, achunks):
    zn, zh, cnt, n = s.zn, s.zh, s.count, s.n
    plan.add(p + "part", (zh, 2, 2, cnt, width), BF16)
    plan.add(p + "near", (zh, 2, cnt, width - bwidth), BF16)
    plan.add(p + "mid", (zh, 2, cnt, width - bwidth), BF16)
    plan.add(p + "far", (zn - 1, cnt, width - bwidth), BF16)
    plan.add(p + "b1", (zh, 2, cnt, bwidth), BF16)
    plan.add(p + "b2", (zh, 2, cnt, bwidth), BF16)
    plan.add(p + "b3", (zh, cnt, bwidth), BF16)
    plan.add(p + "b4", (zh, cnt, bwidth), BF16)
    plan.add(p + "b5", (max(1, zh - 1), cnt, bwidth), BF16)
    plan.add(p + "side", (n, cnt, LANES), F32)
    plan.add(p + "sides", (n - 1, cnt, LANES), F32)
    for k in "sr":
        plan.sem(p + "x" + k, achunks)
        plan.sem(p + "z" + k, achunks, zn - 1)
        plan.sem(p + "p" + k)
        plan.sem(p + "q" + k)
        plan.sem(p + "c" + k, max(1, zh - 1))
        plan.sem(p + "e" + k, n - 1)


def add_spread(plan, s, p, width, achunks, with_b):
    plan.add(p + "hid", (s.zh, 2, 2, s.count, width), BF16)
    for k in "sr":
        plan.sem(p + "h" + k, achunks, s.zn - 1)
        plan.sem(p + "g" + k, achunks)
        if with_b:
            plan.sem(p + "i" + k, max(1, s.zh - 1))
            plan.sem(p + "j" + k)
            plan.sem(p + "k" + k)


def add_finish(plan, s, p, last):
    plan.add(p + "acc", (s.rows, s.depth), F32)
    if last and not s.split:
        plan.add(p + "t0", (s.nt, s.rows, s.depth // s.nt), BF16)
        plan.add(p + "t1", (s.nt - 1, s.rows, s.depth // s.nt), BF16)
        for k in "sr":
            plan.sem(p + "t" + k, s.nt - 1)
        return
    plan.add(p + "t0", (2, s.half, s.depth), BF16)
    plan.add(p + "t1", (s.half, s.depth), BF16)
    plan.add(p + "t2", (s.half, s.depth), BF16)
    plan.add(p + "t3", (max(1, s.ny - 1), s.half, s.depth), BF16)
    plan.add(p + "feat", (2, s.half, s.depth), BF16)
    for k in "sr":
        plan.sem(p + "t" + k)
        plan.sem(p + "u" + k, max(1, s.ny - 1))
        plan.sem(p + "v" + k)


def make_plan(s, weights):
    plan = Plan()
    for name, shape, dtype in weights:
        plan.add("v_" + name, shape, dtype)
    plan.sem("w", len(weights))
    plan.sem("w1", 2, len(s.ff_a) + 1)
    plan.add("feat", (2, s.half, s.depth), BF16)
    plan.add("gains", (s.nt, 3, s.depth // s.nt) if not s.split else (1, 3, s.depth), F32)
    plan.sem("l0", 4)
    for k in "sr":
        plan.sem("f" + k, s.nt - 1)
        plan.sem("n" + k, s.nt - 1)
    fb = (s.ff_b[1] - s.ff_b[0]) * LANES
    for p in ("1", "2"):
        add_sum(plan, s, p, 2 * s.units, 2 * fb, len(s.ff_a))
        add_spread(plan, s, p, s.units, len(s.ff_a), True)
    add_sum(plan, s, "m", s.mix_width, s.mix_b[1] - s.mix_b[0], len(s.mix_a))
    add_spread(plan, s, "m", s.inner, s.groups, False)
    add_finish(plan, s, "1", False)
    add_finish(plan, s, "m", False)
    add_finish(plan, s, "2", True)
    plan.add("proj", (s.count, s.mix_width), F32)
    plan.add("conv", (s.groups, s.count, s.channels), F32)
    plan.add("vecs", (s.groups, s.count, s.state), BF16)
    return plan


class Body:
    def __init__(self, s, r):
        self.s, self.r, self.sent = s, r, []
        me = lax.axis_index("kv")
        self.me, self.z, self.x = me, me // 2, lax.rem(me, 2)
        self.q, self.par = me // 4, lax.rem(me // 2, 2)
        self.tp = lax.axis_index("tp")
        self.y, self.core = self.tp // 2, lax.rem(self.tp, 2)
        self.xpeer = self.z * 2 + 1 - self.x
        self.ppeer = (self.q * 2 + 1 - self.par) * 2 + self.x

    def start(self, copy):
        copy.start()
        self.sent.append(copy)
        return copy

    def send(self, src, dst, sem, *index, **where):
        s, r = self.r[sem + "s"], self.r[sem + "r"]
        index = index or (0,)
        return self.start(copy_to(src, dst, s.at[index], r.at[index], **where))

    def local(self, src, dst, sem):
        copy = pltpu.make_async_copy(src, dst, sem)
        copy.start()
        return copy

    def side_send(self, p):
        side, sides = self.r[p + "side"], self.r[p + "sides"]
        self.sides = []
        for d in range(1, self.s.n):
            k = lax.rem(self.me + d, self.s.n)
            self.sides.append(self.send(side.at[k], sides.at[d - 1], p + "e", d - 1, kv=k))

    def side_total(self, p):
        total = self.r[p + "side"][self.me]
        for d, copy in enumerate(self.sides):
            copy.wait_recv()
            total = total + self.r[p + "sides"][d]
        return total

    def x_send(self, p, c, lo, hi):
        cols = pl.ds(lo, hi - lo)
        r = self.r
        return self.send(
            r[p + "part"].at[:, :, 1 - self.x, :, cols], r[p + "near"].at[:, :, :, cols], p + "x", c, kv=self.xpeer
        )

    def z_send(self, p, c, lo, hi, copy):
        cols = pl.ds(lo, hi - lo)
        r, s = self.r, self.s
        copy.wait_recv()
        total = r[p + "part"][:, :, self.x, :, cols].astype(F32) + r[p + "near"][:, :, :, cols].astype(F32)
        r[p + "mid"][:, :, :, cols] = total.astype(BF16)
        copies = []
        for d in range(1, s.zn):
            zp = lax.rem(self.z + d, s.zn)
            copies.append(
                self.send(
                    r[p + "mid"].at[zp // 2, lax.rem(zp, 2), :, cols],
                    r[p + "far"].at[d - 1, :, cols],
                    p + "z", c, d - 1, kv=zp * 2 + self.x,
                )
            )
        return copies

    def z_total(self, p, lo, hi, copies):
        cols = pl.ds(lo, hi - lo)
        r = self.r
        total = r[p + "mid"][self.q, self.par, :, cols].astype(F32)
        for d, copy in enumerate(copies):
            copy.wait_recv()
            total = total + r[p + "far"][d, :, cols].astype(F32)
        return total

    def p_send(self, p, lo, hi):
        r = self.r
        cols = pl.ds(lo, hi - lo)
        return self.send(r[p + "part"].at[:, 1 - self.par, :, :, cols], r[p + "b1"], p + "p", kv=self.ppeer)

    def q_send(self, p, lo, hi, copy):
        r = self.r
        copy.wait_recv()
        total = r[p + "part"][:, self.par, :, :, pl.ds(lo, hi - lo)].astype(F32) + r[p + "b1"][...].astype(F32)
        r[p + "b2"][...] = total.astype(BF16)
        return self.send(r[p + "b2"].at[:, 1 - self.x], r[p + "b3"], p + "q", kv=self.xpeer)

    def c_send(self, p, copy):
        r, s = self.r, self.s
        copy.wait_recv()
        total = r[p + "b2"][:, self.x].astype(F32) + r[p + "b3"][...].astype(F32)
        r[p + "b4"][...] = total.astype(BF16)
        copies = []
        for d in range(1, s.zh):
            qp = lax.rem(self.q + d, s.zh)
            copies.append(
                self.send(
                    r[p + "b4"].at[qp], r[p + "b5"].at[d - 1], p + "c", d - 1, kv=(qp * 2 + self.par) * 2 + self.x
                )
            )
        return copies

    def c_total(self, p, copies):
        r = self.r
        total = r[p + "b4"][self.q].astype(F32)
        for d, copy in enumerate(copies):
            copy.wait_recv()
            total = total + r[p + "b5"][d].astype(F32)
        return total

    def spot(self, p, z, cols):
        return self.r[p + "hid"].at[z // 2, lax.rem(z, 2), self.x, :, cols]

    def h_send(self, p, c, cols):
        s = self.s
        mine = self.spot(p, self.z, cols)
        for d in range(1, s.zn):
            zp = lax.rem(self.z + d, s.zn)
            self.send(mine, mine, p + "h", c, d - 1, kv=zp * 2 + self.x)

    def arrived(self, place, sem, *index, **where):
        index = index or (0,)
        copy_to(place, place, self.r[sem + "s"].at[index], self.r[sem + "r"].at[index], **where).wait_recv()

    def g_send(self, p, c, cols):
        s = self.s
        for d in range(1, s.zn):
            left = lax.rem(self.z - d + s.zn, s.zn)
            self.arrived(self.spot(p, left, cols), p + "h", c, d - 1, kv=left * 2 + self.x)
        block = self.r[p + "hid"].at[:, :, self.x, :, cols]
        self.send(block, block, p + "g", c, kv=self.xpeer)

    def g_wait(self, p, c, cols):
        self.arrived(self.r[p + "hid"].at[:, :, 1 - self.x, :, cols], p + "g", c, kv=self.xpeer)

    def i_send(self, p, cols):
        s = self.s
        mine = self.spot(p, self.z, cols)
        for d in range(1, s.zh):
            qp = lax.rem(self.q + d, s.zh)
            self.send(mine, mine, p + "i", d - 1, kv=(qp * 2 + self.par) * 2 + self.x)

    def j_send(self, p, cols):
        s = self.s
        for d in range(1, s.zh):
            left = lax.rem(self.q - d + s.zh, s.zh) * 2 + self.par
            self.arrived(self.spot(p, left, cols), p + "i", d - 1, kv=left * 2 + self.x)
        block = self.r[p + "hid"].at[:, self.par, self.x, :, cols]
        self.send(block, block, p + "j", kv=self.xpeer)

    def k_send(self, p, cols):
        hid = self.r[p + "hid"]
        self.arrived(hid.at[:, self.par, 1 - self.x, :, cols], p + "j", kv=self.xpeer)
        block = hid.at[:, self.par, :, :, cols]
        self.send(block, block, p + "k", kv=self.ppeer)

    def k_wait(self, p, cols):
        self.arrived(self.r[p + "hid"].at[:, 1 - self.par, :, :, cols], p + "k", kv=self.ppeer)

    def finish(self, p, weight, before):
        r, s = self.r, self.s
        t0, t1, t2, t3, feat = (r[p + k] for k in ("t0", "t1", "t2", "t3", "feat"))
        t0[...] = r[p + "acc"][...].astype(BF16).reshape(2, s.half, s.depth)
        other = self.tp + 1 - 2 * self.core
        copy = self.send(t0.at[1 - self.core], t1, p + "t", tp=other)
        copy.wait_recv()
        t2[...] = (t0[self.core].astype(F32) + t1[...].astype(F32)).astype(BF16)
        copies = []
        for d in range(1, s.ny):
            yp = lax.rem(self.y + d, s.ny)
            copies.append(self.send(t2, t3.at[d - 1], p + "u", d - 1, tp=yp * 2 + self.core))
        total = t2[...].astype(F32)
        for d, copy in enumerate(copies):
            copy.wait_recv()
            total = total + t3[d].astype(F32)
        feat[self.core] = (before[self.core].astype(F32) + weight * total).astype(BF16)
        mine = feat.at[self.core]
        self.send(mine, mine, p + "v", tp=other)
        self.arrived(feat.at[1 - self.core], p + "v", tp=other)
        return feat

    def finish_last(self, p, weight, before, out_ref):
        r, s = self.r, self.s
        if s.split:
            feat = Body.finish_split(self, p, weight, before)
            out_ref[...] = feat[...].reshape(s.rows, s.depth)
            return
        width = s.depth // s.nt
        t0, t1 = r[p + "t0"], r[p + "t1"]
        for k in range(s.nt):
            t0[k] = r[p + "acc"][:, k * width : (k + 1) * width].astype(BF16)
        copies = []
        for d in range(1, s.nt):
            k = lax.rem(self.tp + d, s.nt)
            copies.append(self.send(t0.at[k], t1.at[d - 1], p + "t", d - 1, tp=k))
        total = t0[self.tp].astype(F32)
        for d, copy in enumerate(copies):
            copy.wait_recv()
            total = total + t1[d].astype(F32)
        cols = pl.ds(pl.multiple_of(self.tp * width, LANES), width)
        mine = before[:, :, cols].astype(F32).reshape(s.rows, width)
        out_ref[...] = (mine + weight * total).astype(BF16)

    def finish_split(self, p, weight, before):
        return self.finish(p, weight, before)

    def gain(self, k):
        gains = self.r["gains"]
        return jnp.concatenate([gains[t, k : k + 1, :] for t in range(gains.shape[0])], axis=1)

    def normed(self, p, feat, k):
        s = self.s
        values = feat[...].reshape(s.rows, s.depth).astype(F32)
        squares = jnp.sum(values * values, axis=1, keepdims=True)
        self.r[p + "side"][...] = jnp.broadcast_to(squares, (s.rows, LANES)).reshape(s.n, s.count, LANES)
        return (values * self.gain(k)).astype(BF16)

    def put_part(self, p, lo, value):
        s = self.s
        w = value.shape[1]
        self.r[p + "part"][:, :, :, :, pl.ds(lo, w)] = value.astype(BF16).reshape(s.zh, 2, 2, s.count, w)

    def feed_forward(self, p, feat, k, ready):
        s, r = self.s, self.r
        gate, up, down = (r["v_" + w + p] for w in ("gate", "up", "down"))
        acc = r[p + "acc"]
        scaled = self.normed(p, feat, k)
        spans = s.ff_a + [s.ff_b]
        b = len(s.ff_a)

        def span(c, scale=1):
            return spans[c][0] * LANES * scale, spans[c][1] * LANES * scale

        def cols(c):
            lo, hi = span(c)
            return pl.ds(lo, hi - lo)

        def multiply(c):
            ready(c)
            lo, hi = span(c)
            for i, w in enumerate((gate, up)):
                value = jnp.dot(scaled, w[:, lo:hi], preferred_element_type=F32)
                self.put_part(p, 2 * lo + i * (hi - lo), value)

        def activate(c, total):
            lo, hi = span(c)
            total = total * self.factor
            hidden = sigmoid_gate(total[:, : hi - lo]) * total[:, hi - lo :]
            r[p + "hid"][self.q, self.par, self.x, :, pl.ds(lo, hi - lo)] = hidden.astype(BF16)

        def lower(c):
            lo, hi = span(c)
            if c < b:
                self.g_wait(p, c, cols(c))
            else:
                self.k_wait(p, cols(c))
            hidden = r[p + "hid"][:, :, :, :, pl.ds(lo, hi - lo)].reshape(s.rows, hi - lo)
            value = jnp.dot(hidden, down[lo:hi, :], preferred_element_type=F32)
            if c == 0:
                acc[...] = value
            else:
                acc[...] += value

        xs, zs = {}, {}
        many = range(b)

        def start(c):
            multiply(c)
            xs[c] = self.x_send(p, c, *span(c, 2))

        def along(c):
            zs[c] = self.z_send(p, c, *span(c, 2), xs[c])

        def spread(c):
            activate(c, self.z_total(p, *span(c, 2), zs[c]))
            self.h_send(p, c, cols(c))

        def forward(c):
            self.g_send(p, c, cols(c))

        start(0)
        multiply(b)
        pair = self.p_send(p, *span(b, 2))
        self.side_send(p)
        for c in many[1:-1]:
            start(c)
        along(0)
        self.factor = None
        second = self.q_send(p, *span(b, 2), pair)
        start(b - 1)
        squares = self.side_total(p)
        self.factor = lax.rsqrt(squares / (s.depth * s.n) + norm_epsilon)[:, :1]
        along(1)
        spread(0)
        along(2)
        cross = self.c_send(p, second)
        spread(1)
        for c in many[3:]:
            along(c)
        forward(0)
        activate(b, self.c_total(p, cross))
        self.i_send(p, cols(b))
        spread(2)
        forward(1)
        for c in many[3:]:
            spread(c)
        self.j_send(p, cols(b))
        forward(2)
        lower(0)
        self.k_send(p, cols(b))
        for c in many[3:]:
            forward(c)
        lower(1)
        lower(2)
        lower(b)
        for c in many[3:]:
            lower(c)

    def mixer(self, p, feat, outs):
        s, r = self.s, self.r
        fresh_ref, si_ref, decay_ref, write_ref = outs
        scaled = self.normed(p, feat, 1)
        side = r[p + "side"]
        spans = s.mix_a + [s.mix_b]
        b = len(s.mix_a)
        proj = r["proj"]

        def multiply(c):
            for name, lo, hi in s.mix_chunks[c]:
                at, w = s.place[name, lo]
                weight = r["v_" + name]
                if name == "step":
                    value = jnp.dot(scaled, weight[...], preferred_element_type=F32)
                    self.put_part(p, at, jnp.zeros((s.rows, LANES), F32))
                    self.put_part(p, at, value)
                else:
                    self.put_part(p, at, jnp.dot(scaled, weight[:, lo:hi], preferred_element_type=F32))

        def keep(c, total):
            lo, hi = spans[c]
            proj[:, lo:hi] = (total * self.factor).astype(BF16).astype(F32)

        xs, zs = {}, {}
        multiply(0)
        xs[0] = self.x_send(p, 0, *spans[0])
        multiply(b)
        pair = self.p_send(p, *spans[b])
        self.side_send(p)
        multiply(1)
        xs[1] = self.x_send(p, 1, *spans[1])
        multiply(2)
        self.conv_past()
        zs[0] = self.z_send(p, 0, *spans[0], xs[0])
        second = self.q_send(p, *spans[b], pair)
        xs[2] = self.x_send(p, 2, *spans[2])
        zs[1] = self.z_send(p, 1, *spans[1], xs[1])
        cross = self.c_send(p, second)
        squares = self.side_total(p)
        self.factor = lax.rsqrt(squares / (s.depth * s.n) + norm_epsilon)[:, :1]
        keep(0, self.z_total(p, *spans[0], zs[0]))
        zs[2] = self.z_send(p, 2, *spans[2], xs[2])
        keep(1, self.z_total(p, *spans[1], zs[1]))
        keep(b, self.c_total(p, cross))
        keep(2, self.z_total(p, *spans[2], zs[2]))

        def take(name):
            pieces = []
            for chunk in s.mix_chunks:
                for other, lo, _ in chunk:
                    if other == name:
                        pieces.append((lo, *s.place[name, lo]))
            return jnp.concatenate([proj[:, at : at + w] for _, at, w in sorted(pieces)], axis=1)

        values, writes, reads = take("value"), take("write"), take("read")
        at, _ = s.place["step", 0]
        steps = proj[:, at : at + LANES][:, : s.heads]
        step = jax.nn.softplus(steps + r["v_bias"][...])
        decay = jnp.exp(-step * jnp.exp(r["v_rate"][...]))
        head_row = lax.broadcasted_iota(jnp.int32, (s.heads, s.inner), 0)
        head_col = lax.broadcasted_iota(jnp.int32, (s.heads, s.inner), 1) // s.head
        widen = (head_row == head_col).astype(F32)
        exact = dict(preferred_element_type=F32, precision=lax.Precision.HIGHEST)
        step_wide = jnp.dot(step, widen, **exact)
        decay_wide = jnp.dot(decay, widen, **exact)
        decay_ref[...] = decay_wide
        gw, st = s.group_width, s.state
        conv_w = r["v_conv_w"]
        taps = conv_w.shape[0]
        gates = take("gate")
        scaled_inputs, lone, activated = [], [], []
        for g in range(s.groups):
            fresh = jnp.concatenate(
                [values[:, g * gw : (g + 1) * gw], writes[:, g * st : (g + 1) * st], reads[:, g * st : (g + 1) * st]],
                axis=1,
            )
            fresh_ref[g] = fresh
            act = sigmoid_gate(r["conv"][g] + fresh * conv_w[taps - 1, g : g + 1, :])
            inputs, write, read = act[:, :gw], act[:, gw : gw + st], act[:, gw + st :]
            si = inputs * step_wide[:, g * gw : (g + 1) * gw]
            si_ref[:, g * gw : (g + 1) * gw] = si
            write_ref[:, g * st : (g + 1) * st] = write
            r["vecs"][g] = read.astype(BF16)
            scaled_inputs.append(si)
            lone.append(jnp.sum(write * read, axis=1, keepdims=True))
        state = r["v_state"]
        per = s.heads // s.groups
        row = lax.broadcasted_iota(jnp.int32, (s.count, s.state), 0)
        for g in range(s.groups):

            def one(k, total, g=g):
                held = state[k, g * per : (g + 1) * per].reshape(gw, st).astype(BF16)
                vec = r["vecs"][g]
                vec = jnp.where(row == k, vec.astype(F32), 0.0).astype(BF16)
                return total + lax.dot_general(
                    vec, held, (((1,), (1,)), ((), ())), preferred_element_type=F32
                )

            drawn = lax.fori_loop(0, s.count, one, jnp.zeros((s.count, gw), F32))
            cols = slice(g * gw, (g + 1) * gw)
            readout = decay_wide[:, cols] * drawn + scaled_inputs[g] * lone[g]
            gated = readout * sigmoid_gate(gates[:, cols])
            mean = jnp.sum(gated * gated, axis=1, keepdims=True) / gw
            mixed = gated * lax.rsqrt(mean + norm_epsilon) * r["v_group_gain"][:, cols]
            r[p + "hid"][self.q, self.par, self.x, :, pl.ds(g * gw, gw)] = mixed.astype(BF16)
            self.h_send(p, g, pl.ds(g * gw, gw))
        for g in range(s.groups):
            self.g_send(p, g, pl.ds(g * gw, gw))
        acc = r[p + "acc"]
        for g in range(s.groups):
            cols = pl.ds(g * gw, gw)
            self.g_wait(p, g, cols)
            mixed = r[p + "hid"][:, :, :, :, cols].reshape(s.rows, gw)
            value = jnp.dot(mixed, r["v_out"][g * gw : (g + 1) * gw, :], preferred_element_type=F32)
            if g == 0:
                acc[...] = value
            else:
                acc[...] += value

    def conv_past(self):
        s, r = self.s, self.r
        past, weight, conv = r["v_conv_state"], r["v_conv_w"], r["conv"]
        taps = weight.shape[0]

        def one(k, carry):
            total = past[k, 0].astype(F32) * weight[0]
            for t in range(1, taps - 1):
                total = total + past[k, t].astype(F32) * weight[t]
            for g in range(s.groups):
                conv[g, pl.ds(k, 1), :] = total[g : g + 1, :]
            return carry

        lax.fori_loop(0, s.count, one, 0)


def step_kernel(s, plan, names, *refs):
    count = len(names)
    hbm = dict(zip(names, refs[:count]))
    outs = refs[count : count + 5]
    r = dict(zip(plan.names, refs[count + 5 :]))
    body = Body(s, r)
    order = [n for n in names if n not in ("stream", "gain1", "gain2", "gain3")]
    gains = r["gains"]
    width = s.depth // s.nt
    spans = s.ff_a + [s.ff_b]
    head = []
    if s.split:
        head.append(body.local(hbm["stream"], r["feat"], r["l0"].at[0]))
        head.append(body.local(hbm["gain1"], gains.at[0], r["l0"].at[1]))
    else:
        mine = pl.ds(pl.multiple_of(body.tp * width, LANES), width)
        head.append(body.local(hbm["stream"], r["feat"].at[:, :, mine], r["l0"].at[0]))
        for k in range(3):
            head.append(body.local(hbm["gain%d" % (k + 1)], gains.at[body.tp, pl.ds(k, 1)], r["l0"].at[k + 1]))
    first = {}
    for c in [0, len(spans) - 1] + list(range(1, len(spans) - 1)):
        lo, hi = spans[c]
        cols = pl.ds(lo * LANES, (hi - lo) * LANES)
        for i, name in enumerate(("gate1", "up1")):
            first[c, i] = body.local(hbm[name].at[:, cols], r["v_" + name].at[:, cols], r["w1"].at[i, c])
    sem = pltpu.get_barrier_semaphore()
    for d in range(1, s.n):
        pl.semaphore_signal(sem, inc=1, device_id={"kv": lax.rem(body.me + d, s.n)}, device_id_type=MESH)
    for d in range(1, s.nt):
        pl.semaphore_signal(sem, inc=1, device_id={"tp": lax.rem(body.tp + d, s.nt)}, device_id_type=MESH)
    pl.semaphore_wait(sem, s.n + s.nt - 2)
    for copy in head:
        copy.wait()
    if not s.split:
        block = r["feat"].at[:, :, mine]
        for d in range(1, s.nt):
            k = lax.rem(body.tp + d, s.nt)
            body.send(block, block, "f", d - 1, tp=k)
            body.send(gains.at[body.tp], gains.at[body.tp], "n", d - 1, tp=k)
        for d in range(1, s.nt):
            left = lax.rem(body.tp - d + s.nt, s.nt)
            place = r["feat"].at[:, :, pl.ds(pl.multiple_of(left * width, LANES), width)]
            body.arrived(place, "f", d - 1, tp=left)
            body.arrived(gains.at[left], "n", d - 1, tp=left)
    rest = {}

    def ready(c):
        first[c, 0].wait()
        first[c, 1].wait()
        if c == 0:
            for i, name in enumerate(order):
                if name not in ("gate1", "up1"):
                    rest[name] = body.local(hbm[name], r["v_" + name], r["w"].at[i])

    waited = set()

    def need(*wanted):
        for name in wanted:
            if name not in waited:
                waited.add(name)
                rest[name].wait()

    plain_lower = body.g_wait

    def g_wait(p, c, cols):
        plain_lower(p, c, cols)
        need({"1": "down1", "2": "down2", "m": "out"}[p])

    body.g_wait = g_wait
    body.feed_forward("1", r["feat"], 0, ready)
    after = body.finish("1", 0.5, r["feat"])
    need("value", "write", "read", "step", "gate", "bias", "rate", "conv_w", "group_gain", "conv_state", "state")
    body.mixer("m", after, outs[1:])
    after = body.finish("m", 1.0, after)
    need("gate2", "up2")
    body.feed_forward("2", after, 2, lambda c: None)
    body.finish_last("2", 0.5, after, outs[0])
    for copy in body.sent:
        copy.wait_send()


def update_kernel(s, block, state_ref, past_ref, fresh_ref, si_ref, decay_ref, write_ref, next_ref, *rest):
    state_out, past_out, next_out, left_ref = rest
    cnt, gw, st = s.count, s.group_width, s.state

    @pl.when(pl.program_id(0) == 0)
    def prepare():
        next_out[...] = next_ref[...]
        for g in range(s.groups):
            cols = slice(g * gw, (g + 1) * gw)
            si, decay = si_ref[:, cols], decay_ref[:, cols]
            high = si.astype(BF16).astype(F32)
            low = si - high
            d1 = decay.astype(BF16).astype(F32)
            d2 = (decay - d1).astype(BF16).astype(F32)
            d3 = decay - d1 - d2
            parts = [high, high, low, d1, d2, d3]
            parts.append(jnp.zeros((left_ref.shape[2] - len(parts) * cnt, gw), F32))
            left_ref[g] = jnp.concatenate(parts, axis=0).T.astype(BF16)

    row = lax.broadcasted_iota(jnp.int32, (cnt, st), 0)

    def one(i, carry):
        k = pl.program_id(0) * block + i
        here = row == k
        pick = jnp.where(here, 1.0, 0.0)
        zero = jnp.zeros((cnt, st), F32)
        per = s.heads // s.groups
        taps = past_ref.shape[1]
        newest = []
        for g in range(s.groups):
            write = jnp.where(here, write_ref[:, g * st : (g + 1) * st], 0.0)
            high = write.astype(BF16).astype(F32)
            low = write - high
            side = jnp.concatenate([high, low, high, zero, zero, zero], axis=0)
            ones = jnp.concatenate([zero, zero, zero, pick, pick, pick], axis=0)
            right = jnp.concatenate([side, ones], axis=1)
            fill = left_ref.shape[2] - right.shape[0]
            right = jnp.concatenate([right, jnp.zeros((fill, 2 * st), F32)], axis=0).astype(BF16)
            both = jnp.dot(left_ref[g], right, preferred_element_type=F32)
            held = state_ref[i, g * per : (g + 1) * per].reshape(gw, st)
            state_out[i, g * per : (g + 1) * per] = (held * both[:, st:] + both[:, :st]).reshape(per, s.head, st)
            newest.append(fresh_ref[g, pl.ds(k, 1), :])
        for t in range(taps - 1):
            past_out[i, t] = past_ref[i, t + 1]
        past_out[i, taps - 1] = jnp.concatenate(newest, axis=0).astype(BF16)
        return carry

    lax.fori_loop(0, block, one, 0)


def gathered(stream, gains):
    n = lax.axis_size("tp")
    features = lax.all_gather(stream, "tp", axis=1, tiled=True)
    packed = lax.all_gather(jnp.stack(gains), "tp", axis=1, tiled=True)
    return features, packed


def on_device(
    stream,
    ssm_state,
    conv_state,
    first_gain,
    first_gate,
    first_up,
    first_down,
    mix_gain,
    gate_in,
    value_in,
    write_in,
    read_in,
    step_in,
    conv_weight,
    step_bias,
    log_decay_rate,
    group_gain,
    out_weight,
    last_norm_gain,
    second_gate,
    second_up,
    second_down,
):
    n, nt = lax.axis_size("kv"), lax.axis_size("tp")
    rows, width = stream.shape
    depth, units = first_gate.shape
    heads, head, state = ssm_state.shape[1:]
    groups = conv_weight.shape[1]
    split = width % LANES != 0
    s = Sizes(n, nt, rows, depth, units, heads, head, state, groups, split)
    if split:
        features, packed = gathered(stream, [first_gain, mix_gain, last_norm_gain])
        named = {"stream": features.reshape(2, s.half, depth), "gain1": packed}
    else:
        named = {
            "stream": stream.reshape(2, s.half, width),
            "gain1": first_gain[None],
            "gain2": mix_gain[None],
            "gain3": last_norm_gain[None],
        }
    weights = {
        "gate1": first_gate,
        "up1": first_up,
        "down1": first_down,
        "value": value_in,
        "gate": gate_in,
        "write": write_in,
        "read": read_in,
        "step": step_in,
        "conv_w": conv_weight,
        "bias": step_bias[None],
        "rate": log_decay_rate[None],
        "group_gain": group_gain[None],
        "conv_state": conv_state,
        "state": ssm_state,
        "out": out_weight,
        "gate2": second_gate,
        "up2": second_up,
        "down2": second_down,
    }
    plan = make_plan(s, [(k, v.shape, v.dtype) for k, v in weights.items()])
    named.update(weights)
    cnt = s.count
    out_width = depth if split else width
    outs = [
        jax.ShapeDtypeStruct((rows, out_width), BF16),
        jax.ShapeDtypeStruct((groups, cnt, s.channels), F32),
        jax.ShapeDtypeStruct((cnt, s.inner), F32),
        jax.ShapeDtypeStruct((cnt, s.inner), F32),
        jax.ShapeDtypeStruct((cnt, groups * state), F32),
    ]
    result, fresh, si, decay, write = pl.pallas_call(
        functools.partial(step_kernel, s, plan, list(named)),
        out_shape=outs,
        in_specs=[HB] * len(named),
        out_specs=[VM] * len(outs),
        scratch_shapes=plan.shapes,
        compiler_params=pltpu.CompilerParams(
            collective_id=0, has_side_effects=True, vmem_limit_bytes=56 * 1024 * 1024
        ),
    )(*named.values())
    if split:
        me = lax.axis_index("tp")
        result = lax.dynamic_slice_in_dim(result, me * width, width, axis=1)
    block = 2
    deep = -(-6 * cnt // LANES) * LANES

    def rows_of(*dims):
        return pl.BlockSpec((block,) + dims, lambda i: (i,) + (0,) * len(dims))

    def whole(array):
        return pl.BlockSpec(array.shape, lambda i: (0,) * array.ndim)

    state_next, past_next, stream_next = pl.pallas_call(
        functools.partial(update_kernel, s, block),
        grid=(cnt // block,),
        out_shape=[
            jax.ShapeDtypeStruct(ssm_state.shape, ssm_state.dtype),
            jax.ShapeDtypeStruct(conv_state.shape, conv_state.dtype),
            jax.ShapeDtypeStruct(stream.shape, BF16),
        ],
        in_specs=[rows_of(*ssm_state.shape[1:]), rows_of(*conv_state.shape[1:])]
        + [whole(a) for a in (fresh, si, decay, write, result)],
        out_specs=[rows_of(*ssm_state.shape[1:]), rows_of(*conv_state.shape[1:]), whole(stream)],
        scratch_shapes=[pltpu.VMEM((groups, s.group_width, deep), BF16)],
        compiler_params=pltpu.CompilerParams(vmem_limit_bytes=60 * 1024 * 1024),
    )(ssm_state, conv_state, fresh, si, decay, write, result)
    return (stream_next, state_next, past_next)


def solution(mesh):
    return jax.shard_map(
        on_device,
        mesh=mesh,
        in_specs=(
            P(None, ("kv", "tp")),
            P("kv", "tp", None, None),
            P("kv", None, "tp", None),
            P(("kv", "tp")),
            P("kv", "tp"),
            P("kv", "tp"),
            P("tp", "kv"),
            P(("kv", "tp")),
            P("kv", "tp"),
            P("kv", "tp"),
            P("kv", "tp"),
            P("kv", "tp"),
            P("kv", "tp"),
            P(None, "tp", None),
            P("tp"),
            P("tp"),
            P("tp"),
            P("tp", "kv"),
            P(("kv", "tp")),
            P("kv", "tp"),
            P("kv", "tp"),
            P("tp", "kv"),
        ),
        out_specs=(P(None, ("kv", "tp")), P("kv", "tp", None, None), P("kv", None, "tp", None)),
        check_vma=False,
    )
```

time: 178 us -> 133 us (0.75)
  matrix products: 20.8 us -> 0 us
  other arithmetic: 12.4 us -> 0 us
  local copies, waits for them, and re-layouts: 9.15 us -> 1.48 us
  Pallas kernels: 134 us -> 130 us
    dot_general x13 -> x0, matrix products: 20.8 us -> none  [the longest x1 5.84 us: token_mixer(): jnp.einsum('bghpn,bgn->bghp', updated, read_vec)]
    add x1 -> x0, other arithmetic: 8.37 us -> none  [token_mixer(): carried * decay[:, :, :, None, None]]
    unnamed x40 -> x1, local copies, waits for them, and re-layouts: 6 us -> 1.48 us
    pallas_call x8 -> x2, Pallas kernels: 134 us -> 130 us  [the longest x1 119 us: on_device(): pl.pallas_call(functools.partial(step_kernel, s, plan, list(named)), out_...]
where the time goes in v1:
time: 133 us; the launch traced here: 132 us
  Pallas kernels  130 us (98%)
  local copies, waits for them, and re-layouts  1.48 us (1%)
    pallas_call x1, Pallas kernels, on_device(): pl.pallas_call(functools.partial(step_kernel, s, plan, list(named)), out_...  119 us
    pallas_call x1, Pallas kernels, on_device(): pl.pallas_call(functools.partial(update_kernel, s, block), grid=(cnt // b...  10.9 us

profile of v1, /device:TPU:0, one launch (start us, length us, event | category | flops | bytes accessed | tf_op | source)
XLA Modules:
  0.0 132.4 jit_solution(17421116974079129046)
XLA Ops:
  0.6 1.5 %copy.25.refs_11_ = bf16[512,16]{1,0:T(8,128)(2,1)} copy(bf16[512,16]{0,1:T(8,128)(2,1)} %param.34) | data formatting | bytes 32768 | tf_op args[12]
  2.1 119.3 %shard_map.229 = (bf16[128,128]{1,0:T(8,128)(2,1)}, f32[2,16,768]{2,1,0:T(8,128)}, f32[16,1024]{1,0:T(8,128)}, f32[16,1024]{1,0:T(8,128)}, f32[16,256]{1,0:T(8,128)}) custom-call(bf16[2,64,128]{2,1,0:T(8,128)(2,1)} %bitcast.7, f32[1,128]{1,0:T(1,128)} %bitcast.9, f32[1,128]{1,0:T(1,128)} %bitcast.10, f32[1,128]{1,0:T(1,128)} %bitcast.11, ...), custom_call_target="tpu_custom_call" | custom-call | tf_op jit(solution)/shard_map/pallas_call | solution.py:822
  121.5 10.9 %shard_map.230 = (f32[16,16,64,128]{3,2,1,0:T(8,128)}, bf16[16,3,2,768]{3,2,1,0:T(2,128)(2,1)}, bf16[128,128]{1,0:T(8,128)(2,1)}) custom-call(f32[16,16,64,128]{3,2,1,0:T(8,128)} %state_ref.1, bf16[16,3,2,768]{3,2,1,0:T(2,128)(2,1)} %past_ref.1, f32[2,16,768]{2,1,0:T(8,128)} %get-tuple-element.11.fresh_ref, f32[16,1024]{1,0:T(8,128)} %get-tuple-element.12.si_ref, ...), custom_call_target="tpu_custom_call" | custom-call | tf_op jit(solution)/shard_map/pallas_call | solution.py:844

commit v2 on v1

v2 whole, which is shorter than its diff:
```python
import functools

import jax
import jax.numpy as jnp
from jax import lax
from jax.experimental import pallas as pl
from jax.experimental.pallas import tpu as pltpu
from jax.sharding import PartitionSpec as P

norm_epsilon = 1e-06
MESH = pl.DeviceIdType.MESH
LANES = 128
KV, TP = "kv", "tp"
DIRECT, THREE, FIRST = "d", "t", "f"
VM = pl.BlockSpec(memory_space=pltpu.VMEM)
HB = pl.BlockSpec(memory_space=pltpu.HBM)
F32 = jnp.float32
BF16 = jnp.bfloat16


def sigmoid_gate(v):
    return v / (1.0 + jnp.exp(-v))


def copy_to(src, dst, send, recv, **where):
    return pltpu.make_async_remote_copy(
        src_ref=src, dst_ref=dst, send_sem=send, recv_sem=recv, device_id=where, device_id_type=MESH
    )


def tag(p, stage, c):
    return p + stage + str(c)


class Plan:
    def __init__(self):
        self.names, self.shapes = [], []

    def add(self, name, shape, dtype):
        self.names.append(name)
        self.shapes.append(pltpu.VMEM(shape, dtype))

    def sem(self, name, *shape):
        self.names.append(name)
        self.shapes.append(pltpu.SemaphoreType.DMA(shape or (1,)))


def cut(total, shares):
    ends = [0] + [max(1, round(total * s)) for s in shares] + [total]
    return [(a, b) for a, b in zip(ends, ends[1:]) if b > a]


SUM = {DIRECT: "xz", THREE: "xpc", FIRST: "pxc"}
SPREAD = {DIRECT: "hg", THREE: "ijg", FIRST: "ijk"}
FF_CHUNKS = [(DIRECT, THREE, 4), (FIRST, FIRST, 6), (THREE, THREE, 7), (THREE, DIRECT, 5)]
MIX_WAYS = (DIRECT, FIRST, DIRECT, DIRECT)
PARTS, UPDATE, UPDATES = 2, 8, 4
ORDER = [
    10010, 10, 0, 20, 30, 1, 11, 10000, 21, 2, 31, 10020, 10030, 12,
    10011, 22, 10001, 13, 32, 3, 10021, 23, 10031, 10012, 10002, 4, 33, 10022,
    14, 24, 10032, 10003, 5, 15, 34, 10013, 25, 10023, 10033, 10004, 10014, 35,
    16, 10024, 26, 1000, 1001, 10034, 10005, 10015, 10025, 1002, 10035, 10016, 1003, 2000,
    10026, 11000, 2010, 2020, 2030, 11001, 2001, 2011, 2021, 11002, 2031, 11003, 12020, 12000,
    12010, 2012, 2032, 2022, 12001, 12021, 12030, 2002, 12011, 2013, 3000, 12031, 8010, 8030,
    8020, 12012, 4001, 4011, 12022, 12032, 12002, 8000, 12013, 13000, 4002, 4012, 5000, 5001,
    18000, 18020, 18030, 14001, 14011, 5002, 18010, 5003, 6000, 6020, 6010, 14012, 14002, 15000,
    6030, 15001, 6001, 15002, 6011, 6021, 15003, 16010, 16000, 6002, 16020, 6012, 6031, 16030,
    6022, 16011, 16001, 6032, 6003, 6013, 16021, 6023, 16031, 16002, 16012, 6033, 6004, 16022,
    6014, 16032, 6024, 16003, 6005, 6015, 16013, 6034, 16023, 6025, 16004, 16033, 6016, 16014,
    16024, 6035, 6026, 16034, 7000, 16015, 16025, 16005, 16016, 16035, 16026, 17000, 7001, 17001,
]


class Sizes:
    def __init__(self, n, nt, rows, depth, units, heads, head, state, groups, split):
        self.n, self.nt, self.rows, self.depth, self.units = n, nt, rows, depth, units
        self.heads, self.head, self.state, self.groups, self.split = heads, head, state, groups, split
        self.zn, self.zh, self.ny = n // 2, n // 4, nt // 2
        self.parts = PARTS
        self.all_rows, self.rows = rows, rows // PARTS
        self.count, self.half = self.rows // n, self.rows // 2
        self.deep = -(-3 * self.count // LANES) * LANES
        tiles = units // LANES
        shares = [share for _, _, share in FF_CHUNKS]
        ends = [sum(shares[: i + 1]) / sum(shares) for i in range(len(shares) - 1)]
        self.ff_chunks = [
            (out, back, a * LANES, z * LANES) for (out, back, _), (a, z) in zip(FF_CHUNKS, cut(tiles, ends))
        ]
        self.inner = heads * head
        self.group_width = self.inner // groups
        self.channels = self.group_width + 2 * state
        v = self.inner // LANES
        vec = groups * state
        gb = max(1, v * 5 // 8)
        self.mix_chunks = [
            [("value", 0, v // 2 * LANES)],
            [("gate", 0, gb * LANES)],
            [("value", v // 2 * LANES, v * LANES), ("write", 0, vec)],
            [("read", 0, vec), ("step", 0, LANES), ("gate", gb * LANES, v * LANES)],
        ]
        spans, at = [], 0
        self.place = {}
        for chunk in self.mix_chunks:
            lo = at
            for name, a, z in chunk:
                self.place[name, a] = (at, z - a)
                at += z - a
            spans.append((lo, at))
        self.mix_spans = [(way, None, a, z) for way, (a, z) in zip(MIX_WAYS, spans)]
        self.mix_width = at


def add_sum(plan, s, p, width, chunks):
    zn, zh, cnt, n = s.zn, s.zh, s.count, s.n
    zl = max(1, zh - 1)
    plan.add(p + "part", (zh, 2, 2, cnt, width), BF16)
    plan.add(p + "near", (zh, 2, cnt, width), BF16)
    plan.add(p + "mid", (zh, 2, cnt, width), BF16)
    plan.add(p + "far", (zn - 1, cnt, width), BF16)
    plan.add(p + "near2", (zh, cnt, width), BF16)
    plan.add(p + "mid2", (zh, cnt, width), BF16)
    plan.add(p + "far2", (zl, cnt, width), BF16)
    plan.add(p + "side", (n, s.count, LANES), F32)
    plan.add(p + "sides", (n - 1, s.count, LANES), F32)
    plan.sem(p + "e")
    for c, chunk in enumerate(chunks):
        for stage in SUM[chunk[0]]:
            plan.sem(p + stage + str(c))


def add_spread(plan, s, p, width, chunks):
    plan.add(p + "hid", (s.zh, 2, 2, s.count, width), BF16)
    for c, chunk in enumerate(chunks):
        for stage in SPREAD[chunk[1]]:
            plan.sem(p + stage + str(c))


def add_finish(plan, s, p, last):
    plan.add(p + "acc", (s.rows, s.depth), F32)
    if last and not s.split:
        plan.add(p + "t0", (s.nt, s.rows, s.depth // s.nt), BF16)
        plan.add(p + "t1", (s.nt - 1, s.rows, s.depth // s.nt), BF16)
        plan.sem(p + "t")
        return
    plan.add(p + "t0", (2, s.half, s.depth), BF16)
    plan.add(p + "t1", (s.half, s.depth), BF16)
    plan.add(p + "t2", (s.half, s.depth), BF16)
    plan.add(p + "t3", (max(1, s.ny - 1), s.half, s.depth), BF16)
    plan.add(p + "feat", (2, s.half, s.depth), BF16)
    for stage in "tuv":
        plan.sem(p + stage)


def make_plan(s, weights):
    plan = Plan()
    for name, shape, dtype in weights:
        if name != "state":
            plan.add("v_" + name, shape, dtype)
    plan.sem("w", len(weights))
    plan.sem("w1", 2, len(s.ff_chunks))
    plan.add("feat", (s.n, s.parts, s.count, s.depth), BF16)
    plan.add("gains", (s.nt, 3, s.depth // s.nt) if not s.split else (1, 3, s.depth), F32)
    plan.sem("l0", 4)
    plan.sem("sent")
    plan.sem("f")
    plan.sem("n")
    for part in range(s.parts):
        q = str(part)
        plan.add("b" + q, (2, s.half, s.depth), BF16)
        for p in ("1" + q, "2" + q):
            add_sum(plan, s, p, 2 * s.units, s.ff_chunks)
            add_spread(plan, s, p, s.units, s.ff_chunks)
        add_sum(plan, s, "m" + q, s.mix_width, s.mix_spans)
        add_spread(plan, s, "m" + q, s.inner, [(DIRECT, DIRECT)] * s.groups)
        add_finish(plan, s, "1" + q, False)
        add_finish(plan, s, "m" + q, False)
        add_finish(plan, s, "2" + q, True)
        plan.add("proj" + q, (s.count, s.mix_width), F32)
        plan.add("conv" + q, (s.groups, s.count, s.channels), F32)
        plan.add("vecs" + q, (s.groups, s.count, s.state), F32)
        plan.add("left" + q, (s.groups, s.group_width, s.deep), BF16)
        plan.add("write" + q, (s.groups, s.count, s.state), F32)
        plan.add("decay" + q, (s.count, s.heads), F32)
    return plan


def scoped(f):
    @functools.wraps(f)
    def inner(*args):
        tag = "_".join(str(a) for a in args if isinstance(a, (str, int)))
        with jax.named_scope(f.__name__ + "_" + tag):
            return f(*args)

    return inner


class Body:
    def __init__(self, s, r, part, sent):
        self.s, self.r, self.sent, self.part, self.tail = s, r, sent, part, str(part)
        self.stage = None
        me = lax.axis_index(KV)
        self.me, self.z, self.x = me, me // 2, lax.rem(me, 2)
        self.q, self.par = me // 4, lax.rem(me // 2, 2)
        self.tp = lax.axis_index(TP)
        self.y, self.core = self.tp // 2, lax.rem(self.tp, 2)
        self.xpeer = self.z * 2 + 1 - self.x
        self.ppeer = (self.q * 2 + 1 - self.par) * 2 + self.x

    def start(self, copy):
        copy.start()
        self.sent.append(copy)
        return copy

    def send(self, src, dst, sem, **where):
        return self.start(copy_to(src, dst, self.r["sent"].at[0], self.r[sem].at[0], **where))

    def came(self, place, sem):
        pltpu.make_async_copy(place, place, self.r[sem].at[0]).wait()

    def local(self, src, dst, sem):
        copy = pltpu.make_async_copy(src, dst, sem)
        copy.start()
        return copy

    @scoped
    def side_send(self, p):
        side, sides = self.r[p + "side"], self.r[p + "sides"]
        for d in range(1, self.s.n):
            k = lax.rem(self.me + d, self.s.n)
            self.send(side.at[k], sides.at[d - 1], p + "e", kv=k)

    @scoped
    def row_factor(self, p):
        s = self.s
        total = self.r[p + "side"][self.me]
        self.came(self.r[p + "sides"], p + "e")
        for d in range(s.n - 1):
            total = total + self.r[p + "sides"][d]
        return lax.rsqrt(total / (s.depth * s.n) + norm_epsilon)[:, :1]

    def columns(self, chunk, scale=1):
        return pl.ds(chunk[2] * scale, (chunk[3] - chunk[2]) * scale)

    def across(self, q):
        return (q * 2 + self.par) * 2 + self.x

    def sum_start(self, p, c, kind, cols):
        part, near = self.r[p + "part"], self.r[p + "near"].at[:, :, :, cols]
        if kind == FIRST:
            self.send(part.at[:, 1 - self.par, :, :, cols], near, tag(p, "p", c), kv=self.ppeer)
        else:
            self.send(part.at[:, :, 1 - self.x, :, cols], near, tag(p, "x", c), kv=self.xpeer)

    @scoped
    def sum_step(self, p, name, c, kind, cols):
        r, s = self.r, self.s
        part, near, mid = r[p + "part"], r[p + "near"], r[p + "mid"]
        near2, mid2 = r[p + "near2"], r[p + "mid2"]
        sem = tag(p, name, c)
        if name == "c":
            kept = mid[:, self.x, :, cols] if kind == FIRST else mid[:, self.par, :, cols]
            self.came(near2.at[:, :, cols], tag(p, "x" if kind == FIRST else "p", c))
            mid2[:, :, cols] = (kept.astype(F32) + near2[:, :, cols].astype(F32)).astype(BF16)
            for d in range(1, s.zh):
                q = lax.rem(self.q + d, s.zh)
                self.send(mid2.at[q, :, cols], r[p + "far2"].at[d - 1, :, cols], sem, kv=self.across(q))
            return
        self.came(near.at[:, :, :, cols], tag(p, "p" if kind == FIRST else "x", c))
        kept = part[:, self.par, :, :, cols] if kind == FIRST else part[:, :, self.x, :, cols]
        mid[:, :, :, cols] = (kept.astype(F32) + near[:, :, :, cols].astype(F32)).astype(BF16)
        if name == "z":
            for d in range(1, s.zn):
                z = lax.rem(self.z + d, s.zn)
                src = mid.at[z // 2, lax.rem(z, 2), :, cols]
                self.send(src, r[p + "far"].at[d - 1, :, cols], sem, kv=z * 2 + self.x)
        elif name == "p":
            self.send(mid.at[:, 1 - self.par, :, cols], near2.at[:, :, cols], sem, kv=self.ppeer)
        else:
            self.send(mid.at[:, 1 - self.x, :, cols], near2.at[:, :, cols], sem, kv=self.xpeer)

    @scoped
    def sum_total(self, p, c, kind, cols):
        r = self.r
        if kind == DIRECT:
            own, far, sem = r[p + "mid"].at[self.q, self.par], r[p + "far"], tag(p, "z", c)
        else:
            own, far, sem = r[p + "mid2"].at[self.q], r[p + "far2"], tag(p, "c", c)
        total = own[:, cols].astype(F32)
        self.came(far.at[:, :, cols], sem)
        for d in range(far.shape[0]):
            total = total + far[d, :, cols].astype(F32)
        return total

    def spot(self, p, z, cols):
        return self.r[p + "hid"].at[z // 2, lax.rem(z, 2), self.x, :, cols]

    def spread_start(self, p, c, kind, cols):
        s = self.s
        mine = self.spot(p, self.z, cols)
        if kind == DIRECT:
            for d in range(1, s.zn):
                z = lax.rem(self.z + d, s.zn)
                self.send(mine, mine, tag(p, "h", c), kv=z * 2 + self.x)
        else:
            for d in range(1, s.zh):
                self.send(mine, mine, tag(p, "i", c), kv=self.across(lax.rem(self.q + d, s.zh)))

    @scoped
    def spread_step(self, p, name, c, kind, cols):
        r = self.r
        hid = r[p + "hid"]
        first = kind == FIRST
        if name == "g" and kind == DIRECT:
            self.came(r[p + "far"].at[:, :, cols], tag(p, "h", c))
        elif name == "j":
            self.came(r[p + "far2"].at[:, :, cols], tag(p, "i", c))
        elif name == "g":
            self.came(hid.at[:, 1 - self.par, self.x, :, cols], tag(p, "j", c))
        else:
            self.came(hid.at[:, self.par, 1 - self.x, :, cols], tag(p, "j", c))
        if name == "j":
            own = hid.at[:, self.par, self.x, :, cols]
            self.send(own, own, tag(p, "j", c), kv=self.xpeer if first else self.ppeer)
        elif name == "g":
            own = hid.at[:, :, self.x, :, cols]
            self.send(own, own, tag(p, "g", c), kv=self.xpeer)
        else:
            own = hid.at[:, self.par, :, :, cols]
            self.send(own, own, tag(p, "k", c), kv=self.ppeer)

    @scoped
    def spread_end(self, p, c, kind, cols):
        hid = self.r[p + "hid"]
        if kind == FIRST:
            self.came(hid.at[:, 1 - self.par, :, :, cols], tag(p, "k", c))
        else:
            self.came(hid.at[:, :, 1 - self.x, :, cols], tag(p, "g", c))
        self.need("out" if p[0] == "m" else "down" + p[0])

    @scoped
    def finish_core(self, p):
        r, s = self.r, self.s
        t0 = r[p + "t0"]
        t0[...] = r[p + "acc"][...].astype(BF16).reshape(2, s.half, s.depth)
        self.send(t0.at[1 - self.core], r[p + "t1"], p + "t", tp=self.tp + 1 - 2 * self.core)

    @scoped
    def finish_y(self, p):
        r, s = self.r, self.s
        t2 = r[p + "t2"]
        self.came(r[p + "t1"], p + "t")
        t2[...] = (r[p + "t0"][self.core].astype(F32) + r[p + "t1"][...].astype(F32)).astype(BF16)
        for d in range(1, s.ny):
            yp = lax.rem(self.y + d, s.ny)
            self.send(t2, r[p + "t3"].at[d - 1], p + "u", tp=yp * 2 + self.core)

    @scoped
    def finish_rows(self, p, weight, before):
        r, s = self.r, self.s
        t3, feat = r[p + "t3"], r[p + "feat"]
        total = r[p + "t2"][...].astype(F32)
        self.came(t3, p + "u")
        for d in range(s.ny - 1):
            total = total + t3[d].astype(F32)
        feat[self.core] = (before[self.core].astype(F32) + weight * total).astype(BF16)
        mine = feat.at[self.core]
        self.send(mine, mine, p + "v", tp=self.tp + 1 - 2 * self.core)

    @scoped
    def finish_end(self, p):
        feat = self.r[p + "feat"]
        self.came(feat.at[1 - self.core], p + "v")
        return feat

    def finish(self, p, weight, before, k):
        if k == 0:
            self.finish_core(p)
        elif k == 1:
            self.finish_y(p)
        elif k == 2:
            self.finish_rows(p, weight, before)
        else:
            self.finish_end(p)

    @scoped
    def last_start(self, p):
        r, s = self.r, self.s
        width = s.depth // s.nt
        t0, t1 = r[p + "t0"], r[p + "t1"]
        for k in range(s.nt):
            t0[k] = r[p + "acc"][:, k * width : (k + 1) * width].astype(BF16)
        for d in range(1, s.nt):
            k = lax.rem(self.tp + d, s.nt)
            self.send(t0.at[k], t1.at[d - 1], p + "t", tp=k)

    @scoped
    def last_end(self, p, weight, before, out_ref):
        r, s = self.r, self.s
        width = s.depth // s.nt
        t1 = r[p + "t1"]
        total = r[p + "t0"][self.tp].astype(F32)
        self.came(t1, p + "t")
        for d in range(s.nt - 1):
            total = total + t1[d].astype(F32)
        cols = pl.ds(pl.multiple_of(self.tp * width, LANES), width)
        mine = before[:, :, cols].astype(F32).reshape(s.rows, width)
        out_ref[:, self.part] = (mine + weight * total).reshape(s.n, s.count, width).astype(BF16)

    def finish_last(self, p, weight, before, out_ref, k):
        s = self.s
        if s.split:
            for j in (2 * k, 2 * k + 1):
                self.finish(p, weight, before, j)
            if k == 1:
                feat = self.r[p + "feat"][...].astype(F32)
                out_ref[:, self.part] = feat.reshape(s.n, s.count, s.depth).astype(BF16)
        elif k == 0:
            self.last_start(p)
        else:
            self.last_end(p, weight, before, out_ref)

    def gain(self, k):
        gains = self.r["gains"]
        return jnp.concatenate([gains[t, k : k + 1, :] for t in range(gains.shape[0])], axis=1)

    @scoped
    def normed(self, p, feat, k):
        s = self.s
        values = feat[...].astype(F32).reshape(s.rows, s.depth)
        squares = jnp.sum(values * values, axis=1, keepdims=True)
        self.r[p + "side"][...] = jnp.broadcast_to(squares, (s.rows, LANES)).reshape(s.n, s.count, LANES)
        return (values * self.gain(k)).astype(BF16)

    def put_part(self, p, lo, value):
        s = self.s
        w = value.shape[1]
        self.r[p + "part"][:, :, :, :, pl.ds(lo, w)] = value.reshape(s.zh, 2, 2, s.count, w).astype(BF16)

    def event(self, stage, c, k):
        s, r, q = self.s, self.r, self.tail
        before = (r["b" + q], r["1" + q + "feat"], r["m" + q + "feat"])
        if stage == UPDATE:
            self.update(c * s.count // UPDATES, (c + 1) * s.count // UPDATES)
        elif stage in (0, 6):
            self.feed_forward(("1" if stage == 0 else "2") + q, before[stage // 3], stage // 3, c, k)
        elif stage == 1:
            self.finish("1" + q, 0.5, before[0], k)
        elif stage == 2:
            self.project("m" + q, before[1], c, k)
        elif stage == 3:
            self.mix("m" + q)
        elif stage == 4 and c < s.groups:
            self.mixed("m" + q, c, k)
        elif stage == 5:
            self.finish("m" + q, 1.0, before[1], k)
        elif stage == 7:
            self.finish_last("2" + q, 0.5, before[2], self.outs["next"], k)

    def begin(self, p, feat, k):
        if self.stage != p:
            self.scaled, self.factor, self.lowered = self.normed(p, feat, k), None, False
            self.stage, self.started = p, 0
        self.started += 1

    @scoped
    def multiply(self, p, c):
        r = self.r
        if p[0] == "1":
            self.ready(c)
        else:
            self.need("gate2", "up2")
        _, _, lo, hi = self.s.ff_chunks[c]
        for i, w in enumerate(("gate", "up")):
            weight = r["v_" + w + p[0]]
            self.put_part(p, 2 * lo + i * (hi - lo), jnp.dot(self.scaled, weight[:, lo:hi], preferred_element_type=F32))

    def activated(self, p, c, way, cols):
        total = self.sum_total(p, c, way, cols)
        if self.factor is None:
            self.factor = self.row_factor(p)
        return total * self.factor

    @scoped
    def lower(self, p, name, c, lo, hi):
        s, r = self.s, self.r
        hidden = r[p + "hid"][:, :, :, :, pl.ds(lo, hi - lo)].astype(F32).reshape(s.rows, hi - lo)
        weight = r["v_" + name]
        value = jnp.dot(hidden.astype(BF16), weight[lo:hi, :], preferred_element_type=F32)
        if not self.lowered:
            r[p + "acc"][...] = value
        else:
            r[p + "acc"][...] += value
        self.lowered = True

    def feed_forward(self, p, feat, gain, c, k):
        chunk = self.s.ff_chunks[c]
        way, back, lo, hi = chunk
        there, home = SUM[way], SPREAD[back]
        cols, wide = self.columns(chunk), self.columns(chunk, 2)
        at = k - len(there)
        if k == 0:
            self.begin(p, feat, gain)
            self.multiply(p, c)
            self.sum_start(p, c, way, wide)
            if self.started == 2:
                self.side_send(p)
        elif at < 0:
            self.sum_step(p, there[k], c, way, wide)
        elif at == 0:
            total = self.activated(p, c, way, wide)
            hidden = sigmoid_gate(total[:, : hi - lo]) * total[:, hi - lo :]
            self.r[p + "hid"][self.q, self.par, self.x, :, cols] = hidden.astype(BF16)
            self.spread_start(p, c, back, cols)
        elif at < len(home):
            self.spread_step(p, home[at], c, back, cols)
        else:
            self.spread_end(p, c, back, cols)
            self.lower(p, "down" + p[0], c, lo, hi)

    @scoped
    def multiply_mixer(self, p, c):
        s, r = self.s, self.r
        for name, lo, hi in s.mix_chunks[c]:
            at, w = s.place[name, lo]
            weight = r["v_" + name]
            if name == "step":
                value = lax.dot_general(
                    self.scaled, weight[...], (((1,), (1,)), ((), ())), preferred_element_type=F32
                )
                self.put_part(p, at, jnp.zeros((s.rows, LANES), F32))
                self.put_part(p, at, value)
            else:
                self.put_part(p, at, jnp.dot(self.scaled, weight[:, lo:hi], preferred_element_type=F32))

    def project(self, p, feat, c, k):
        s, r = self.s, self.r
        chunk = s.mix_spans[c]
        way, _, lo, hi = chunk
        cols = self.columns(chunk)
        if k == 0:
            self.need("value", "write", "read", "step", "gate", "bias", "rate", "cw", "gg", "past")
            self.begin(p, feat, 1)
            self.multiply_mixer(p, c)
            self.sum_start(p, c, way, cols)
            if self.started == 2:
                self.side_send(p)
            if c == 2:
                self.conv_past()
        elif k < len(SUM[way]):
            self.sum_step(p, SUM[way][k], c, way, cols)
        else:
            r["proj" + self.tail][:, lo:hi] = self.activated(p, c, way, cols).astype(BF16).astype(F32)

    def mixed(self, p, g, k):
        gw = self.s.group_width
        cols = pl.ds(g * gw, gw)
        if k == 1:
            self.spread_step(p, "g", g, DIRECT, cols)
        else:
            self.spread_end(p, g, DIRECT, cols)
            self.lower(p, "out", g, g * gw, (g + 1) * gw)

    @scoped
    def mix(self, p):
        s, r, q = self.s, self.r, self.tail
        base = self.part * s.count
        proj, fresh_ref = r["proj" + q], self.outs["fresh"]
        self.lowered = False

        def take(name):
            pieces = []
            for chunk in s.mix_chunks:
                for other, lo, _ in chunk:
                    if other == name:
                        pieces.append((lo, *s.place[name, lo]))
            return jnp.concatenate([proj[:, at : at + w] for _, at, w in sorted(pieces)], axis=1)

        values, writes, reads = take("value"), take("write"), take("read")
        at, _ = s.place["step", 0]
        steps = proj[:, at : at + LANES][:, : s.heads]
        step = jax.nn.softplus(steps + r["v_bias"][...])
        decay = jnp.exp(-step * jnp.exp(r["v_rate"][...]))
        head_row = lax.broadcasted_iota(jnp.int32, (s.heads, s.inner), 0)
        head_col = lax.broadcasted_iota(jnp.int32, (s.heads, s.inner), 1) // s.head
        widen = (head_row == head_col).astype(F32)
        exact = dict(preferred_element_type=F32, precision=lax.Precision.HIGHEST)
        step_wide = jnp.dot(step, widen, **exact)
        decay_wide = jnp.dot(decay, widen, **exact)
        r["decay" + q][...] = decay
        gw, st = s.group_width, s.state
        conv_w = r["v_cw"]
        taps = conv_w.shape[0]
        gates = take("gate")
        scaled_inputs, lone, activated = [], [], []
        for g in range(s.groups):
            fresh = jnp.concatenate(
                [values[:, g * gw : (g + 1) * gw], writes[:, g * st : (g + 1) * st], reads[:, g * st : (g + 1) * st]],
                axis=1,
            )
            fresh_ref[g, base : base + s.count, :] = fresh
            act = sigmoid_gate(r["conv" + q][g] + fresh * conv_w[taps - 1, g : g + 1, :])
            inputs, write, read = act[:, :gw], act[:, gw : gw + st], act[:, gw + st :]
            si = inputs * step_wide[:, g * gw : (g + 1) * gw]
            r["write" + q][g] = write
            r["vecs" + q][g] = read
            scaled_inputs.append(si)
            lone.append(jnp.sum(write * read, axis=1, keepdims=True))
        state = r["v_state"]
        per = s.heads // s.groups
        row = lax.broadcasted_iota(jnp.int32, (s.count, s.state), 0)
        self.need("state")

        def one(k, totals):
            found = []
            for g, total in enumerate(totals):
                held = state[base + k, g * per : (g + 1) * per].reshape(gw, st).astype(BF16)
                vec = jnp.where(row == k, r["vecs" + q][g], 0.0).astype(BF16)
                drawn = lax.dot_general(vec, held, (((1,), (1,)), ((), ())), preferred_element_type=F32)
                found.append(total + drawn)
            return tuple(found)

        drawn = lax.fori_loop(
            0, s.count, one, tuple(jnp.zeros((s.count, gw), F32) for _ in range(s.groups)), unroll=4
        )
        whole = [pl.ds(g * gw, gw) for g in range(s.groups)]
        for g in range(s.groups):
            cols = slice(g * gw, (g + 1) * gw)
            readout = decay_wide[:, cols] * drawn[g] + scaled_inputs[g] * lone[g]
            gated = readout * sigmoid_gate(gates[:, cols])
            mean = jnp.sum(gated * gated, axis=1, keepdims=True) / gw
            mixed = gated * lax.rsqrt(mean + norm_epsilon) * r["v_gg"][:, cols]
            r[p + "hid"][self.q, self.par, self.x, :, whole[g]] = mixed.astype(BF16)
            self.spread_start(p, g, DIRECT, whole[g])
        for g in range(s.groups):
            si = scaled_inputs[g]
            high = si.astype(BF16).astype(F32)
            fill = jnp.zeros((s.deep - 3 * s.count, gw), F32)
            r["left" + q][g] = jnp.concatenate([high, high, si - high, fill], axis=0).T.astype(BF16)

    @scoped
    def update(self, lo, hi):
        s, r = self.s, self.r
        q, first = self.tail, self.part * s.count
        state, left, gw, st = r["v_state"], r["left" + q], s.group_width, s.state
        per, block = s.heads // s.groups, 2
        row = lax.broadcasted_iota(jnp.int32, (s.count, st), 0)

        def one(j, carry):
            base = j * block
            for g in range(s.groups):
                write = r["write" + q][g]
                picked = jnp.concatenate([jnp.where(row == base + i, write, 0.0) for i in range(block)], axis=1)
                high = picked.astype(BF16).astype(F32)
                fill = jnp.zeros((s.deep - 3 * s.count, block * st), F32)
                right = jnp.concatenate([high, picked - high, high, fill], axis=0).astype(BF16)
                outer = jnp.dot(left[g], right, preferred_element_type=F32)
                for i in range(block):
                    decay = r["decay" + q][pl.ds(base + i, 1), :]
                    for h in range(g * per, (g + 1) * per):
                        at = (h - g * per) * s.head
                        new = outer[at : at + s.head, i * st : (i + 1) * st]
                        state[first + base + i, h] = state[first + base + i, h] * decay[:, h : h + 1] + new
            return carry

        lax.fori_loop(lo // block, hi // block, one, 0)

    @scoped
    def conv_past(self):
        s, r = self.s, self.r
        past, weight, conv = r["v_past"], r["v_cw"], r["conv" + self.tail]
        first = self.part * s.count
        taps = weight.shape[0]

        def one(k, carry):
            total = past[first + k, 0].astype(F32) * weight[0]
            for t in range(1, taps - 1):
                total = total + past[first + k, t].astype(F32) * weight[t]
            for g in range(s.groups):
                conv[g, pl.ds(k, 1), :] = total[g : g + 1, :]
            return carry

        lax.fori_loop(0, s.count, one, 0)


def step_kernel(s, plan, names, *refs):
    count = len(names)
    hbm = dict(zip(names, refs[:count]))
    outs = dict(zip(("next", "fresh", "state"), refs[count : count + 3]))
    r = dict(zip(plan.names, refs[count + 3 :]))
    r["v_state"] = outs["state"]
    sent = []
    bodies = [Body(s, r, part, sent) for part in range(s.parts)]
    body = bodies[0]
    order = [n for n in names if n not in ("stream", "gain1", "gain2", "gain3")]
    gains = r["gains"]
    width = s.depth // s.nt
    head = []
    if s.split:
        head.append(body.local(hbm["stream"], r["feat"], r["l0"].at[0]))
        head.append(body.local(hbm["gain1"], gains.at[0], r["l0"].at[1]))
    else:
        mine = pl.ds(pl.multiple_of(body.tp * width, LANES), width)
        head.append(body.local(hbm["stream"], r["feat"].at[:, :, :, mine], r["l0"].at[0]))
        for k in range(3):
            head.append(body.local(hbm["gain%d" % (k + 1)], gains.at[body.tp, pl.ds(k, 1)], r["l0"].at[k + 1]))
    sem = pltpu.get_barrier_semaphore()
    for d in range(1, s.n):
        pl.semaphore_signal(sem, inc=1, device_id={KV: lax.rem(body.me + d, s.n)}, device_id_type=MESH)
    for d in range(1, s.nt):
        pl.semaphore_signal(sem, inc=1, device_id={TP: lax.rem(body.tp + d, s.nt)}, device_id_type=MESH)
    for copy in head:
        copy.wait()
    first = {}
    for c in range(len(s.ff_chunks)):
        cols = body.columns(s.ff_chunks[c])
        for i, name in enumerate(("gate1", "up1")):
            first[c, i] = body.local(hbm[name].at[:, cols], r["v_" + name].at[:, cols], r["w1"].at[i, c])
    pl.semaphore_wait(sem, s.n + s.nt - 2)
    if not s.split:
        block = r["feat"].at[:, :, :, mine]
        for d in range(1, s.nt):
            k = lax.rem(body.tp + d, s.nt)
            body.send(block, block, "f", tp=k)
            body.send(gains.at[body.tp], gains.at[body.tp], "n", tp=k)
        body.came(r["feat"].at[:, :, :, pl.ds(0, (s.nt - 1) * width)], "f")
        body.came(gains.at[pl.ds(0, s.nt - 1)], "n")
    rest = {}
    begun = set()

    def ready(c):
        if c in begun:
            return
        first[c, 0].wait()
        first[c, 1].wait()
        if not begun:
            for i, name in enumerate(order):
                if name not in ("gate1", "up1"):
                    rest[name] = body.local(hbm[name], r["v_" + name], r["w"].at[i])
        begun.add(c)

    waited = set()

    def need(*wanted):
        for name in wanted:
            if name not in waited:
                waited.add(name)
                rest[name].wait()

    for body in bodies:
        body.need, body.ready, body.outs = need, ready, outs
        rows = r["feat"][:, body.part].astype(F32)
        r["b" + body.tail][...] = rows.reshape(2, s.half, s.depth).astype(BF16)
    for code in ORDER:
        bodies[code // 10000].event(code // 1000 % 10, code // 10 % 100, code % 10)
    for copy in sent:
        copy.wait_send()


def write_kernel(s, blocks, past_ref, fresh_ref, next_ref, state_ref, state_out, past_out, next_out, sem):
    taps = past_ref.shape[1]
    count = past_ref.shape[0]
    step = count // blocks
    copies = []
    for k in range(blocks):
        rows = pl.ds(k * step, step)
        copy = pltpu.make_async_copy(state_ref.at[rows], state_out.at[rows], sem.at[k])
        copy.start()
        copies.append(copy)
    next_out[...] = next_ref[...]

    def one(k, carry):
        for t in range(taps - 1):
            past_out[k, t] = past_ref[k, t + 1]
        newest = [fresh_ref[g, pl.ds(k, 1), :] for g in range(s.groups)]
        past_out[k, taps - 1] = jnp.concatenate(newest, axis=0).astype(BF16)
        return carry

    lax.fori_loop(0, count, one, 0)
    for copy in copies:
        copy.wait()


def gathered(stream, gains):
    n = lax.axis_size(TP)
    features = lax.all_gather(stream, TP, axis=1, tiled=True)
    packed = lax.all_gather(jnp.stack(gains), TP, axis=1, tiled=True)
    return features, packed


def on_device(
    stream,
    ssm_state,
    constate,
    first_gain,
    first_gate,
    first_up,
    first_down,
    mix_gain,
    gate_in,
    value_in,
    write_in,
    read_in,
    step_in,
    conv_weight,
    step_bias,
    log_decay_rate,
    group_gain,
    out_weight,
    last_norm_gain,
    second_gate,
    second_up,
    second_down,
):
    n, nt = lax.axis_size(KV), lax.axis_size(TP)
    rows, width = stream.shape
    depth, units = first_gate.shape
    heads, head, state = ssm_state.shape[1:]
    groups = conv_weight.shape[1]
    split = width % LANES != 0
    s = Sizes(n, nt, rows, depth, units, heads, head, state, groups, split)
    if split:
        features, packed = gathered(stream, [first_gain, mix_gain, last_norm_gain])
        named = {"stream": features.reshape(n, s.parts, s.count, depth), "gain1": packed}
    else:
        named = {
            "stream": stream.reshape(n, s.parts, s.count, width),
            "gain1": first_gain[None],
            "gain2": mix_gain[None],
            "gain3": last_norm_gain[None],
        }
    weights = {
        "gate1": first_gate,
        "up1": first_up,
        "down1": first_down,
        "value": value_in,
        "gate": gate_in,
        "write": write_in,
        "read": read_in,
        "step": step_in.T,
        "cw": conv_weight,
        "bias": step_bias[None],
        "rate": log_decay_rate[None],
        "gg": group_gain[None],
        "past": constate,
        "state": ssm_state,
        "out": out_weight,
        "gate2": second_gate,
        "up2": second_up,
        "down2": second_down,
    }
    plan = make_plan(s, [(k, v.shape, v.dtype) for k, v in weights.items()])
    named.update(weights)
    result, fresh, held = pl.pallas_call(
        functools.partial(step_kernel, s, plan, list(named)),
        out_shape=[
            pltpu.VMEM((n, s.parts, s.count, depth if split else width), BF16),
            pltpu.VMEM((groups, rows // n, s.channels), F32),
            pltpu.VMEM(ssm_state.shape, ssm_state.dtype),
        ],
        in_specs=[HB] * len(named),
        out_specs=[VM] * 3,
        scratch_shapes=plan.shapes,
        compiler_params=pltpu.CompilerParams(
            collective_id=0, has_side_effects=True, vmem_limit_bytes=48 * 1024 * 1024
        ),
    )(*named.values())
    if split:
        me = lax.axis_index(TP)
        result = lax.dynamic_slice_in_dim(result, me * width, width, axis=3)
    blocks = 8
    state_next, past_next, stream_next = pl.pallas_call(
        functools.partial(write_kernel, s, blocks),
        out_shape=[
            jax.ShapeDtypeStruct(ssm_state.shape, ssm_state.dtype),
            jax.ShapeDtypeStruct(constate.shape, constate.dtype),
            jax.ShapeDtypeStruct(result.shape, BF16),
        ],
        in_specs=[VM] * 4,
        out_specs=[HB, VM, VM],
        scratch_shapes=[pltpu.SemaphoreType.DMA((blocks,))],
        compiler_params=pltpu.CompilerParams(vmem_limit_bytes=8 * 1024 * 1024),
    )(constate, fresh, result, held)
    return (stream_next.reshape(stream.shape), state_next, past_next)


def solution(mesh):
    return jax.shard_map(
        on_device,
        mesh=mesh,
        in_specs=(
            P(None, (KV, TP)),
            P(KV, TP, None, None),
            P(KV, None, TP, None),
            P((KV, TP)),
            P(KV, TP),
            P(KV, TP),
            P(TP, KV),
            P((KV, TP)),
            P(KV, TP),
            P(KV, TP),
            P(KV, TP),
            P(KV, TP),
            P(KV, TP),
            P(None, TP, None),
            P(TP),
            P(TP),
            P(TP),
            P(TP, KV),
            P((KV, TP)),
            P(KV, TP),
            P(KV, TP),
            P(TP, KV),
        ),
        out_specs=(P(None, (KV, TP)), P(KV, TP, None, None), P(KV, None, TP, None)),
        check_vma=False,
    )
```

time: 133 us -> 108 us (0.81)
  Pallas kernels: 130 us -> 107 us
  local copies, waits for them, and re-layouts: 1.48 us -> 0.01 us
    pallas_call x1, Pallas kernels: 119 us -> 103 us  [on_device(): pl.pallas_call(functools.partial(step_kernel, s, plan, list(named)), out_...]
    pallas_call x1, Pallas kernels: 10.9 us -> 4.03 us  [on_device(): pl.pallas_call(functools.partial(write_kernel, s, blocks), out_shape=[jax...]
    unnamed x1 -> x2, local copies, waits for them, and re-layouts: 1.48 us -> 0.01 us
where the time goes in v2:
time: 108 us
  Pallas kernels  107 us (99%)
    pallas_call x1, Pallas kernels, on_device(): pl.pallas_call(functools.partial(step_kernel, s, plan, list(named)), out_...  103 us
    pallas_call x1, Pallas kernels, on_device(): pl.pallas_call(functools.partial(write_kernel, s, blocks), out_shape=[jax...  4.03 us

profile of v2, /device:TPU:0, one launch (start us, length us, event | category | flops | bytes accessed | tf_op | source)
XLA Modules:
  0.0 108.1 jit_solution(13371763828169202942)
XLA Ops:
  0.6 0.0 copy-start
  0.7 103.4 %shard_map.229 = (bf16[8,2,8,128]{3,2,1,0:T(8,128)(2,1)S(1)}, f32[2,16,768]{2,1,0:T(8,128)S(1)}, f32[16,16,64,128]{3,2,1,0:T(8,128)S(1)}) custom-call(bf16[8,2,8,128]{3,2,1,0:T(8,128)(2,1)} %bitcast.9, f32[1,128]{1,0:T(1,128)} %bitcast.12, f32[1,128]{1,0:T(1,128)} %bitcast.13, f32[1,128]{1,0:T(1,128)} %bitcast.14, bf16[512,2816]{1,0:T(8,128)(2,1)} %refs_4_.1, ...), custom_call_target="tpu_custom_call" | custom-call | tf_op jit(solution)/shard_map/pallas_call | solution.py:853
  104.0 0.0 copy-done
  104.0 4.0 %shard_map.230 = (f32[16,16,64,128]{3,2,1,0:T(8,128)}, bf16[16,3,2,768]{3,2,1,0:T(2,128)(2,1)}, bf16[8,2,8,128]{3,2,1,0:T(8,128)(2,1)}) custom-call(bf16[16,3,2,768]{3,2,1,0:T(2,128)(2,1)S(1)} %copy-done, f32[2,16,768]{2,1,0:T(8,128)S(1)} %get-tuple-element.9.fresh_ref, bf16[8,2,8,128]{3,2,1,0:T(8,128)(2,1)S(1)} %get-tuple-element.10.next_ref, ...), custom_call_target="tpu_custom_call" | custom-call | tf_op jit(solution)/shard_map/pallas_call | solution.py:871
Async XLA Ops:
  0.6 103.4 %copy-start = (bf16[16,3,2,768]{3,2,1,0:T(2,128)(2,1)S(1)}, bf16[16,3,2,768]{3,2,1,0:T(2,128)(2,1)}, u32[]{:S(2)}) copy-start(bf16[16,3,2,768]{3,2,1,0:T(2,128)(2,1)} %past_ref.1) | copy-start | bytes 442372

commit v3 on v2

--- a/solution.py
+++ b/solution.py
@@ -52,22 +52,22 @@
 
 SUM = {DIRECT: "xz", THREE: "xpc", FIRST: "pxc"}
 SPREAD = {DIRECT: "hg", THREE: "ijg", FIRST: "ijk"}
-FF_CHUNKS = [(DIRECT, THREE, 4), (FIRST, FIRST, 6), (THREE, THREE, 7), (THREE, DIRECT, 5)]
+FF_CHUNKS = [(DIRECT, THREE, 4), (FIRST, FIRST, 6), (THREE, DIRECT, 6), (THREE, DIRECT, 6)]
 MIX_WAYS = (DIRECT, FIRST, DIRECT, DIRECT)
 PARTS, UPDATE, UPDATES = 2, 8, 4
 ORDER = [
-    10010, 10, 0, 20, 30, 1, 11, 10000, 21, 2, 31, 10020, 10030, 12,
-    10011, 22, 10001, 13, 32, 3, 10021, 23, 10031, 10012, 10002, 4, 33, 10022,
-    14, 24, 10032, 10003, 5, 15, 34, 10013, 25, 10023, 10033, 10004, 10014, 35,
-    16, 10024, 26, 1000, 1001, 10034, 10005, 10015, 10025, 1002, 10035, 10016, 1003, 2000,
-    10026, 11000, 2010, 2020, 2030, 11001, 2001, 2011, 2021, 11002, 2031, 11003, 12020, 12000,
-    12010, 2012, 2032, 2022, 12001, 12021, 12030, 2002, 12011, 2013, 3000, 12031, 8010, 8030,
-    8020, 12012, 4001, 4011, 12022, 12032, 12002, 8000, 12013, 13000, 4002, 4012, 5000, 5001,
-    18000, 18020, 18030, 14001, 14011, 5002, 18010, 5003, 6000, 6020, 6010, 14012, 14002, 15000,
-    6030, 15001, 6001, 15002, 6011, 6021, 15003, 16010, 16000, 6002, 16020, 6012, 6031, 16030,
-    6022, 16011, 16001, 6032, 6003, 6013, 16021, 6023, 16031, 16002, 16012, 6033, 6004, 16022,
-    6014, 16032, 6024, 16003, 6005, 6015, 16013, 6034, 16023, 6025, 16004, 16033, 6016, 16014,
-    16024, 6035, 6026, 16034, 7000, 16015, 16025, 16005, 16016, 16035, 16026, 17000, 7001, 17001,
+    0, 10, 20, 30, 1, 11, 10010, 10000, 21, 10020, 2, 31, 12, 10030,
+    22, 10011, 10001, 32, 10021, 3, 13, 23, 10002, 10031, 10012, 33, 4, 10022,
+    14, 10032, 24, 10003, 5, 10013, 15, 34, 10023, 10004, 25, 10033, 10014, 16,
+    35, 1000, 10024, 10034, 10015, 1001, 10005, 10025, 1002, 10035, 10016, 11000, 2000, 2020,
+    2010, 2030, 11001, 2001, 2011, 2021, 11002, 12010, 12000, 12020, 2031, 2012, 12011, 2002,
+    2022, 12030, 12021, 12001, 2032, 2013, 3000, 12031, 8030, 8010, 8000, 12012, 4001, 12022,
+    4011, 12002, 12013, 12032, 13000, 4002, 4012, 5000, 14001, 18000, 14011, 5001, 5002, 6000,
+    6020, 14002, 6010, 14012, 15000, 6030, 6001, 15001, 6021, 6011, 15002, 16010, 16000, 16020,
+    8020, 16030, 6002, 6031, 6012, 6022, 16001, 6003, 6032, 16011, 16021, 18010, 18020, 18030,
+    6023, 6013, 16002, 16031, 16012, 6004, 6033, 16022, 6014, 16032, 16003, 6024, 16013, 16023,
+    16004, 16033, 16014, 6034, 6005, 16024, 6015, 16015, 16034, 6025, 16005, 16025, 6016, 6035,
+    7000, 16016, 16035, 17000, 7001, 17001,
 ]
 
 
@@ -78,7 +78,7 @@
         self.zn, self.zh, self.ny = n // 2, n // 4, nt // 2
         self.parts = PARTS
         self.all_rows, self.rows = rows, rows // PARTS
-        self.count, self.half = self.rows // n, self.rows // 2
+        self.count = self.rows // n
         self.deep = -(-3 * self.count // LANES) * LANES
         tiles = units // LANES
         shares = [share for _, _, share in FF_CHUNKS]
@@ -142,12 +142,10 @@
         plan.add(p + "t1", (s.nt - 1, s.rows, s.depth // s.nt), BF16)
         plan.sem(p + "t")
         return
-    plan.add(p + "t0", (2, s.half, s.depth), BF16)
-    plan.add(p + "t1", (s.half, s.depth), BF16)
-    plan.add(p + "t2", (s.half, s.depth), BF16)
-    plan.add(p + "t3", (max(1, s.ny - 1), s.half, s.depth), BF16)
-    plan.add(p + "feat", (2, s.half, s.depth), BF16)
-    for stage in "tuv":
+    for name in ("t0", "t1", "t2", "feat"):
+        plan.add(p + name, (s.rows, s.depth), BF16)
+    plan.add(p + "t3", (max(1, s.ny - 1), s.rows, s.depth), BF16)
+    for stage in "uv":
         plan.sem(p + stage)
 
 
@@ -162,11 +160,11 @@
     plan.add("gains", (s.nt, 3, s.depth // s.nt) if not s.split else (1, 3, s.depth), F32)
     plan.sem("l0", 4)
     plan.sem("sent")
-    plan.sem("f")
+    plan.sem("f", s.parts)
     plan.sem("n")
     for part in range(s.parts):
         q = str(part)
-        plan.add("b" + q, (2, s.half, s.depth), BF16)
+        plan.add("b" + q, (s.rows, s.depth), BF16)
         for p in ("1" + q, "2" + q):
             add_sum(plan, s, p, 2 * s.units, s.ff_chunks)
             add_spread(plan, s, p, s.units, s.ff_chunks)
@@ -338,49 +336,25 @@
         self.need("out" if p[0] == "m" else "down" + p[0])
 
     @scoped
-    def finish_core(self, p):
+    def finish(self, p, weight, before, k):
         r, s = self.r, self.s
-        t0 = r[p + "t0"]
-        t0[...] = r[p + "acc"][...].astype(BF16).reshape(2, s.half, s.depth)
-        self.send(t0.at[1 - self.core], r[p + "t1"], p + "t", tp=self.tp + 1 - 2 * self.core)
-
-    @scoped
-    def finish_y(self, p):
-        r, s = self.r, self.s
-        t2 = r[p + "t2"]
-        self.came(r[p + "t1"], p + "t")
-        t2[...] = (r[p + "t0"][self.core].astype(F32) + r[p + "t1"][...].astype(F32)).astype(BF16)
-        for d in range(1, s.ny):
-            yp = lax.rem(self.y + d, s.ny)
-            self.send(t2, r[p + "t3"].at[d - 1], p + "u", tp=yp * 2 + self.core)
-
-    @scoped
-    def finish_rows(self, p, weight, before):
-        r, s = self.r, self.s
-        t3, feat = r[p + "t3"], r[p + "feat"]
-        total = r[p + "t2"][...].astype(F32)
-        self.came(t3, p + "u")
-        for d in range(s.ny - 1):
-            total = total + t3[d].astype(F32)
-        feat[self.core] = (before[self.core].astype(F32) + weight * total).astype(BF16)
-        mine = feat.at[self.core]
-        self.send(mine, mine, p + "v", tp=self.tp + 1 - 2 * self.core)
-
-    @scoped
-    def finish_end(self, p):
-        feat = self.r[p + "feat"]
-        self.came(feat.at[1 - self.core], p + "v")
-        return feat
-
-    def finish(self, p, weight, before, k):
+        t0, t1, t2, t3, feat = (r[p + name] for name in ("t0", "t1", "t2", "t3", "feat"))
         if k == 0:
-            self.finish_core(p)
+            t0[...] = r[p + "acc"][...].astype(BF16)
+            for d in range(1, s.ny):
+                yp = lax.rem(self.y + d, s.ny)
+                self.send(t0, t3.at[d - 1], p + "u", tp=yp * 2 + self.core)
         elif k == 1:
-            self.finish_y(p)
-        elif k == 2:
-            self.finish_rows(p, weight, before)
-        else:
-            self.finish_end(p)
+            total = t0[...].astype(F32)
+            self.came(t3, p + "u")
+            for d in range(s.ny - 1):
+                total = total + t3[d].astype(F32)
+            t2[...] = total.astype(BF16)
+            self.send(t2, t1, p + "v", tp=self.tp + 1 - 2 * self.core)
+        else:
+            self.came(t1, p + "v")
+            total = t2[...].astype(F32) + t1[...].astype(F32)
+            feat[...] = (before[...].astype(F32) + weight * total).astype(BF16)
 
     @scoped
     def last_start(self, p):
@@ -403,13 +377,13 @@
         for d in range(s.nt - 1):
             total = total + t1[d].astype(F32)
         cols = pl.ds(pl.multiple_of(self.tp * width, LANES), width)
-        mine = before[:, :, cols].astype(F32).reshape(s.rows, width)
+        mine = before[:, cols].astype(F32)
         out_ref[:, self.part] = (mine + weight * total).reshape(s.n, s.count, width).astype(BF16)
 
     def finish_last(self, p, weight, before, out_ref, k):
         s = self.s
         if s.split:
-            for j in (2 * k, 2 * k + 1):
+            for j in ((0,), (1, 2))[k]:
                 self.finish(p, weight, before, j)
             if k == 1:
                 feat = self.r[p + "feat"][...].astype(F32)
@@ -426,7 +400,7 @@
     @scoped
     def normed(self, p, feat, k):
         s = self.s
-        values = feat[...].astype(F32).reshape(s.rows, s.depth)
+        values = feat[...].astype(F32)
         squares = jnp.sum(values * values, axis=1, keepdims=True)
         self.r[p + "side"][...] = jnp.broadcast_to(squares, (s.rows, LANES)).reshape(s.n, s.count, LANES)
         return (values * self.gain(k)).astype(BF16)
@@ -457,6 +431,8 @@
             self.finish_last("2" + q, 0.5, before[2], self.outs["next"], k)
 
     def begin(self, p, feat, k):
+        if self.stage is None:
+            self.arrive(self.part)
         if self.stage != p:
             self.scaled, self.factor, self.lowered = self.normed(p, feat, k), None, False
             self.stage, self.started = p, 0
@@ -717,13 +693,25 @@
             first[c, i] = body.local(hbm[name].at[:, cols], r["v_" + name].at[:, cols], r["w1"].at[i, c])
     pl.semaphore_wait(sem, s.n + s.nt - 2)
     if not s.split:
-        block = r["feat"].at[:, :, :, mine]
         for d in range(1, s.nt):
             k = lax.rem(body.tp + d, s.nt)
-            body.send(block, block, "f", tp=k)
             body.send(gains.at[body.tp], gains.at[body.tp], "n", tp=k)
-        body.came(r["feat"].at[:, :, :, pl.ds(0, (s.nt - 1) * width)], "f")
+        parts = sorted(range(s.parts), key=lambda part: part != ORDER[0] // 10000)
+        for part in parts:
+            block = r["feat"].at[:, part, :, mine]
+            for d in range(1, s.nt):
+                k = lax.rem(body.tp + d, s.nt)
+                sent.append(copy_to(block, block, r["sent"].at[0], r["f"].at[part], tp=k))
+                sent[-1].start()
         body.came(gains.at[pl.ds(0, s.nt - 1)], "n")
+
+    def arrive(part):
+        if not s.split:
+            place = r["feat"].at[:, part, :, pl.ds(0, (s.nt - 1) * width)]
+            pltpu.make_async_copy(place, place, r["f"].at[part]).wait()
+        rows = r["feat"][:, part].astype(F32)
+        r["b" + str(part)][...] = rows.reshape(s.rows, s.depth).astype(BF16)
+
     rest = {}
     begun = set()
 
@@ -747,35 +735,33 @@
                 rest[name].wait()
 
     for body in bodies:
-        body.need, body.ready, body.outs = need, ready, outs
-        rows = r["feat"][:, body.part].astype(F32)
-        r["b" + body.tail][...] = rows.reshape(2, s.half, s.depth).astype(BF16)
+        body.need, body.ready, body.outs, body.arrive = need, ready, outs, arrive
     for code in ORDER:
         bodies[code // 10000].event(code // 1000 % 10, code // 10 % 100, code % 10)
     for copy in sent:
         copy.wait_send()
 
 
-def write_kernel(s, blocks, past_ref, fresh_ref, next_ref, state_ref, state_out, past_out, next_out, sem):
-    taps = past_ref.shape[1]
-    count = past_ref.shape[0]
+def write_kernel(s, blocks, past_ref, fresh_ref, next_ref, state_ref, state_out, past_out, next_out, moved, sem):
+    taps, count = past_ref.shape[1], past_ref.shape[0]
     step = count // blocks
-    copies = []
+    copies = [pltpu.make_async_copy(next_ref, next_out, sem.at[blocks])]
     for k in range(blocks):
         rows = pl.ds(k * step, step)
-        copy = pltpu.make_async_copy(state_ref.at[rows], state_out.at[rows], sem.at[k])
+        copies.append(pltpu.make_async_copy(state_ref.at[rows], state_out.at[rows], sem.at[k]))
+    for copy in copies:
         copy.start()
-        copies.append(copy)
-    next_out[...] = next_ref[...]
 
     def one(k, carry):
         for t in range(taps - 1):
-            past_out[k, t] = past_ref[k, t + 1]
+            moved[k, t] = past_ref[k, t + 1]
         newest = [fresh_ref[g, pl.ds(k, 1), :] for g in range(s.groups)]
-        past_out[k, taps - 1] = jnp.concatenate(newest, axis=0).astype(BF16)
+        moved[k, taps - 1] = jnp.concatenate(newest, axis=0).astype(BF16)
         return carry
 
     lax.fori_loop(0, count, one, 0)
+    copies.append(pltpu.make_async_copy(moved, past_out, sem.at[blocks + 1]))
+    copies[-1].start()
     for copy in copies:
         copy.wait()
 
@@ -790,7 +776,7 @@
 def on_device(
     stream,
     ssm_state,
-    constate,
+    conv_state,
     first_gain,
     first_gate,
     first_up,
@@ -841,7 +827,7 @@
         "bias": step_bias[None],
         "rate": log_decay_rate[None],
         "gg": group_gain[None],
-        "past": constate,
+        "past": conv_state,
         "state": ssm_state,
         "out": out_weight,
         "gate2": second_gate,
@@ -872,14 +858,14 @@
         functools.partial(write_kernel, s, blocks),
         out_shape=[
             jax.ShapeDtypeStruct(ssm_state.shape, ssm_state.dtype),
-            jax.ShapeDtypeStruct(constate.shape, constate.dtype),
+            jax.ShapeDtypeStruct(conv_state.shape, conv_state.dtype),
             jax.ShapeDtypeStruct(result.shape, BF16),
         ],
         in_specs=[VM] * 4,
-        out_specs=[HB, VM, VM],
-        scratch_shapes=[pltpu.SemaphoreType.DMA((blocks,))],
+        out_specs=[HB] * 3,
+        scratch_shapes=[pltpu.VMEM(conv_state.shape, BF16), pltpu.SemaphoreType.DMA((blocks + 2,))],
         compiler_params=pltpu.CompilerParams(vmem_limit_bytes=8 * 1024 * 1024),
-    )(constate, fresh, result, held)
+    )(conv_state, fresh, result, held)
     return (stream_next.reshape(stream.shape), state_next, past_next)
 
 

time: 108 us -> 103 us (0.954)
  Pallas kernels: 107 us -> 102 us
    pallas_call x1, Pallas kernels: 103 us -> 98.6 us  [on_device(): pl.pallas_call(functools.partial(step_kernel, s, plan, list(named)), out_...]
where the time goes in v3:
time: 103 us
  Pallas kernels  102 us (99%)
    pallas_call x1, Pallas kernels, on_device(): pl.pallas_call(functools.partial(step_kernel, s, plan, list(named)), out_...  98.6 us
    pallas_call x1, Pallas kernels, on_device(): pl.pallas_call(functools.partial(write_kernel, s, blocks), out_shape=[jax...  3.4 us

profile of v3, /device:TPU:0, one launch (start us, length us, event | category | flops | bytes accessed | tf_op | source)
XLA Modules:
  0.0 102.6 jit_solution(6635377821970103926)
XLA Ops:
  0.6 0.0 copy-start
  0.7 98.6 %shard_map.229 = (bf16[8,2,8,128]{3,2,1,0:T(8,128)(2,1)S(1)}, f32[2,16,768]{2,1,0:T(8,128)S(1)}, f32[16,16,64,128]{3,2,1,0:T(8,128)S(1)}) custom-call(bf16[8,2,8,128]{3,2,1,0:T(8,128)(2,1)} %bitcast.9, f32[1,128]{1,0:T(1,128)} %bitcast.12, f32[1,128]{1,0:T(1,128)} %bitcast.13, f32[1,128]{1,0:T(1,128)} %bitcast.14, bf16[512,2816]{1,0:T(8,128)(2,1)} %refs_4_.1, ...), custom_call_target="tpu_custom_call" | custom-call | tf_op jit(solution)/shard_map/pallas_call | solution.py:839
  99.2 0.0 copy-done
  99.2 3.4 %shard_map.230 = (f32[16,16,64,128]{3,2,1,0:T(8,128)}, bf16[16,3,2,768]{3,2,1,0:T(2,128)(2,1)}, bf16[8,2,8,128]{3,2,1,0:T(8,128)(2,1)}) custom-call(bf16[16,3,2,768]{3,2,1,0:T(2,128)(2,1)S(1)} %copy-done, f32[2,16,768]{2,1,0:T(8,128)S(1)} %get-tuple-element.9.fresh_ref, bf16[8,2,8,128]{3,2,1,0:T(8,128)(2,1)S(1)} %get-tuple-element.10.next_ref, ...), custom_call_target="tpu_custom_call" | custom-call | tf_op jit(solution)/shard_map/pallas_call | solution.py:857
Async XLA Ops:
  0.6 98.6 %copy-start = (bf16[16,3,2,768]{3,2,1,0:T(2,128)(2,1)S(1)}, bf16[16,3,2,768]{3,2,1,0:T(2,128)(2,1)}, u32[]{:S(2)}) copy-start(bf16[16,3,2,768]{3,2,1,0:T(2,128)(2,1)} %past_ref.1) | copy-start | bytes 442372

commit v4 on v3

--- a/solution.py
+++ b/solution.py
@@ -41,6 +41,8 @@
         self.shapes.append(pltpu.VMEM(shape, dtype))
 
     def sem(self, name, *shape):
+        if "1" + name[1:] in self.names and name[0] == "2":
+            return
         self.names.append(name)
         self.shapes.append(pltpu.SemaphoreType.DMA(shape or (1,)))
 
@@ -209,11 +211,14 @@
         self.sent.append(copy)
         return copy
 
+    def sem(self, name):
+        return self.r[name if name in self.r else "1" + name[1:]].at[0]
+
     def send(self, src, dst, sem, **where):
-        return self.start(copy_to(src, dst, self.r["sent"].at[0], self.r[sem].at[0], **where))
+        return self.start(copy_to(src, dst, self.r["sent"].at[0], self.sem(sem), **where))
 
     def came(self, place, sem):
-        pltpu.make_async_copy(place, place, self.r[sem].at[0]).wait()
+        pltpu.make_async_copy(place, place, self.sem(sem)).wait()
 
     def local(self, src, dst, sem):
         copy = pltpu.make_async_copy(src, dst, sem)

time: 103 us -> 102 us (level)
  no operation moved by 1% of the time
where the time goes in v4:
time: 102 us
  Pallas kernels  102 us (100%)
    pallas_call x1, Pallas kernels, on_device(): pl.pallas_call(functools.partial(step_kernel, s, plan, list(named)), out_...  98.2 us
    pallas_call x1, Pallas kernels, on_device(): pl.pallas_call(functools.partial(write_kernel, s, blocks), out_shape=[jax...  3.4 us

profile of v4, /device:TPU:0, one launch (start us, length us, event | category | flops | bytes accessed | tf_op | source)
XLA Modules:
  0.0 102.2 jit_solution(1480445776833693886)
XLA Ops:
  0.6 0.0 copy-start
  0.7 98.2 %shard_map.229 = (bf16[8,2,8,128]{3,2,1,0:T(8,128)(2,1)S(1)}, f32[2,16,768]{2,1,0:T(8,128)S(1)}, f32[16,16,64,128]{3,2,1,0:T(8,128)S(1)}) custom-call(bf16[8,2,8,128]{3,2,1,0:T(8,128)(2,1)} %bitcast.9, f32[1,128]{1,0:T(1,128)} %bitcast.12, f32[1,128]{1,0:T(1,128)} %bitcast.13, f32[1,128]{1,0:T(1,128)} %bitcast.14, bf16[512,2816]{1,0:T(8,128)(2,1)} %refs_4_.1, ...), custom_call_target="tpu_custom_call" | custom-call | tf_op jit(solution)/shard_map/pallas_call | solution.py:844
  98.8 0.0 copy-done
  98.8 3.4 %shard_map.230 = (f32[16,16,64,128]{3,2,1,0:T(8,128)}, bf16[16,3,2,768]{3,2,1,0:T(2,128)(2,1)}, bf16[8,2,8,128]{3,2,1,0:T(8,128)(2,1)}) custom-call(bf16[16,3,2,768]{3,2,1,0:T(2,128)(2,1)S(1)} %copy-done, f32[2,16,768]{2,1,0:T(8,128)S(1)} %get-tuple-element.9.fresh_ref, bf16[8,2,8,128]{3,2,1,0:T(8,128)(2,1)S(1)} %get-tuple-element.10.next_ref, ...), custom_call_target="tpu_custom_call" | custom-call | tf_op jit(solution)/shard_map/pallas_call | solution.py:862
Async XLA Ops:
  0.6 98.2 %copy-start = (bf16[16,3,2,768]{3,2,1,0:T(2,128)(2,1)S(1)}, bf16[16,3,2,768]{3,2,1,0:T(2,128)(2,1)}, u32[]{:S(2)}) copy-start(bf16[16,3,2,768]{3,2,1,0:T(2,128)(2,1)} %past_ref.1) | copy-start | bytes 442372
